TPU v7x, 512 devices: a whole 4x8x8 slice. The times are simulated.
512 devices in a mesh: sp: 32 (over z, x), tp: 16 (over y, core).
Axes of the slice: x: 4, y: 8, z: 8, core: 2. Of those that a mesh axis runs over, the one named last changes fastest.
Arguments:
- query_one: bfloat16 [8192, 1024], P('sp', 'tp'), may hold values from -6 to 6
- key_one: bfloat16 [8192, 1024], P('sp', 'tp'), may hold values from -6 to 6
- value_one: bfloat16 [8192, 2048], P('sp', 'tp'), may hold values from -6 to 6
- gate_one: bfloat16 [8192, 2048], P('sp', 'tp'), may hold values from -6 to 6
- decay_one: float32 [2, 8192, 1024], P(None, 'sp', 'tp')
- query_two: bfloat16 [8192, 2048], P('sp', 'tp'), may hold values from -6 to 6
- key_two: bfloat16 [8192, 2048], P('sp', 'tp'), may hold values from -6 to 6
- value_two: bfloat16 [8192, 2048], P('sp', 'tp'), may hold values from -6 to 6
- gate_two: bfloat16 [8192, 2048], P('sp', 'tp'), may hold values from -6 to 6
- decay_two: float32 [2, 8192, 2048], P(None, 'sp', 'tp')
- head_gain: float32 [128], replicated, may hold values from 0.1 to 1.9
- proj_one: bfloat16 [2048, 2048], P('tp'), may hold values from -0.09375 to 0.09375
- proj_two: bfloat16 [2048, 2048], P('tp'), may hold values from -0.09375 to 0.09375
- stream: bfloat16 [8192, 2048], P('sp'), may hold values from -6 to 6
- gain_mix: float32 [2048], replicated, may hold values from 0.1 to 1.9
- gain_moe: float32 [2048], replicated, may hold values from 0.1 to 1.9
- routes: int32 [8192, 2], P('sp'), may hold values from 0 to 31, all different within a row; in each aligned block of 256 rows (0 to 255, 256 to 511, ...) at most 24 rows name the same one
- affinity: float32 [8192, 2], P('sp'), may hold values from 0.1 to 1
- expert_gate: bfloat16 [32, 2048, 2048], P('sp', None, 'tp'), may hold values from -0.125 to 0.125
- expert_up: bfloat16 [32, 2048, 2048], P('sp', None, 'tp'), may hold values from -0.125 to 0.125
- expert_down: bfloat16 [32, 2048, 2048], P('sp', 'tp'), may hold values from -0.125 to 0.125
Outputs:
- output: bfloat16 [8192, 2048], P(('sp', 'tp'))
Inputs may be any that keep to these rules, and one draw needn't show every extreme that they name: `routes`: in the 256 rows of one index of sp no expert is named more than 24 times, a bound that some block reaches there in every draw; a row names 2 different experts.
All inputs are finite; a program needn't handle non-finite values.
Results may differ from a plain program's by a relative error of at most 0.017.
Values may be sent and summed in bfloat16 or wider, within the bound.
No kernel may reach another device: no remote copies, remote signals or barrier semaphores. Data moves between devices by JAX's collectives and lax.ppermute only.
A program may use at most 64 MiB of HBM per device.

v0:
```python
import jax
import jax.numpy as jnp
from jax import lax
from jax.sharding import Mesh
from jax.sharding import PartitionSpec as P

DK_A = 64
DK_B = 128
BLK = 64
SP = ("sp_0", "sp_1")
SP_TP = ("sp_0", "sp_1", "tp")


normalizer_sharpness = 16.0


def neutral_like(value, identity):
    return jax.tree.map(
        lambda part, zero: jnp.zeros_like(part) + jnp.asarray(zero, part.dtype), value, identity
    )


def gathered_once(value, axis):
    leaves = jax.tree.leaves(value)
    turns = sorted(range(len(leaves)), key=lambda k: -leaves[k].size)
    width = (1, *leaves[turns[0]].shape)[-1]
    lines = [
        jnp.pad(leaves[k].reshape(-1), (0, -leaves[k].size % width)).reshape(-1, width)
        for k in turns
    ]
    both, at, found = (lax.all_gather(jnp.concatenate(lines), axis), 0, {})
    for k, line in zip(turns, lines):
        share = both[:, at : at + len(line)].reshape(len(both), -1)
        found[k] = share[:, : leaves[k].size].reshape(-1, *leaves[k].shape)
        at += len(line)
    numbers = iter(range(len(leaves)))
    return jax.tree.map(lambda _: found[next(numbers)], value)


def carried_in(value, axes, combine, identity, reverse):
    before = start = neutral_like(value, identity)
    total = value
    for axis in reversed(axes):
        peers, mine = (lax.axis_size(axis), lax.axis_index(axis))
        pieces = gathered_once(
            jax.tree.map(
                lambda part, kind: part.astype(kind),
                total,
                jax.tree.map(lambda a: jnp.bfloat16 if a.dtype == jnp.float32 else a.dtype, value),
            ),
            axis,
        )
        inside, total = (start, start)
        for k in reversed(range(peers)) if reverse else range(peers):
            passed = k > mine if reverse else k < mine
            total = combine(
                total, jax.tree.map(lambda part, own: part[k].astype(own.dtype), pieces, value)
            )
            inside = jax.tree.map(lambda new, old: jnp.where(passed, new, old), total, inside)
        before = combine(inside, before)
    return before


def split_up(value, dim, peers):
    before, after = (value.shape[:dim], value.shape[dim + 1 :])
    return jnp.moveaxis(value.reshape(*before, peers, -1, *after), dim, 0)


def summed_on_arrival(value, axis, dim):
    pieces = split_up(value, dim, lax.axis_size(axis))
    arrived = lax.all_to_all(pieces, axis, split_axis=0, concat_axis=0, tiled=True)
    return arrived.astype(jnp.float32).sum(axis=0)


def heads_first(values, heads):
    return values.reshape(values.shape[0], heads, -1).transpose(1, 0, 2)


def block_scan(query, key, value, logarithm_fading):
    heads, length, key_size = query.shape
    value_size = value.shape[-1]
    count = length // BLK

    def blocks(tensor):
        return tensor.reshape(heads, count, BLK, tensor.shape[-1])

    qb, kb, vb, gb = (blocks(query), blocks(key), blocks(value), blocks(logarithm_fading))
    cum = jnp.cumsum(gb, axis=2)
    last = cum[:, :, -1:, :]
    q_in = qb * jnp.exp(cum)
    k_in = kb * jnp.exp(-cum)
    k_st = kb * jnp.exp(last - cum)
    lower = jnp.tril(jnp.ones((BLK, BLK), dtype=bool))
    scores = jnp.where(lower, jnp.einsum("hnid,hnjd->hnij", q_in, k_in), 0.0)
    inner = jnp.einsum("hnij,hnjv->hniv", scores, vb)
    growth = jnp.einsum("hnjd,hnjv->hndv", k_st, vb)
    fading_speed = jnp.exp(last[:, :, 0, :])

    def step(state, inputs):
        factor, added = inputs
        return (factor[..., None] * state + added, state)

    final, starts = lax.scan(
        step,
        jnp.zeros((heads, key_size, value_size), jnp.float32),
        (fading_speed.transpose(1, 0, 2), growth.transpose(1, 0, 2, 3)),
    )
    carried = jnp.einsum("hnid,hndv->hniv", q_in, starts.transpose(1, 0, 2, 3))
    return ((inner + carried).reshape(heads, length, value_size), final)


def group_local(query, key, value, fading_speed, key_size):
    heads = query.shape[1] // key_size
    qh = heads_first(query.astype(jnp.float32), heads) * key_size ** (-0.5)
    kh = heads_first(key.astype(jnp.float32), heads)
    vh = heads_first(value.astype(jnp.float32), heads)
    logarithm_fading = jax.nn.log_sigmoid(fading_speed) / normalizer_sharpness
    ahead = heads_first(logarithm_fading[0], heads)
    behind = heads_first(logarithm_fading[1], heads)[:, ::-1]
    flipped_q = qh[:, ::-1]
    forward, state_ahead = block_scan(qh, kh, vh, ahead)
    backward, state_behind = block_scan(flipped_q, kh[:, ::-1], vh[:, ::-1], behind)
    cum_ahead = jnp.cumsum(ahead, axis=1)
    cum_behind = jnp.cumsum(behind, axis=1)
    reader_ahead = qh * jnp.exp(cum_ahead)
    reader_behind = flipped_q * jnp.exp(cum_behind)
    return (
        forward,
        backward,
        reader_ahead,
        reader_behind,
        cum_ahead[:, -1, :],
        cum_behind[:, -1, :],
        state_ahead,
        state_behind,
    )


def chain(earlier, later):
    return (
        earlier[0] + later[0],
        jnp.exp(later[0])[..., None] * earlier[1] + later[1],
        earlier[2] + later[2],
        jnp.exp(later[2])[..., None] * earlier[3] + later[3],
    )


def readout(reader, state):
    return jnp.einsum("htd,hdv->htv", reader, state)


def finish(mixed, gate, head_gain):
    normed = mixed * lax.rsqrt(jnp.mean(mixed * mixed, axis=-1, keepdims=True) + 1e-06) * head_gain
    flat = normed.transpose(1, 0, 2).reshape(mixed.shape[1], -1)
    return (flat * jax.nn.silu(gate.astype(jnp.float32))).astype(jnp.bfloat16)


def layer_norm(values, gain):
    mean = jnp.mean(values, axis=-1, keepdims=True)
    spread = jnp.mean(jnp.square(values - mean), axis=-1, keepdims=True)
    return (values - mean) * lax.rsqrt(spread + 1e-05) * gain


def body(
    query_one,
    key_one,
    value_one,
    gate_one,
    decay_one,
    query_two,
    key_two,
    value_two,
    gate_two,
    decay_two,
    head_gain,
    proj_one,
    proj_two,
    stream,
    gain_mix,
    gain_moe,
    routes,
    affinity,
    expert_gate,
    expert_up,
    expert_down,
):
    rows = query_one.shape[0]
    tp_count = lax.axis_size("tp")
    tp_rank = lax.axis_index("tp")
    sp_count = lax.axis_size(SP)
    own_rows = rows // tp_count
    first = group_local(query_one, key_one, value_one, decay_one, DK_A)
    second = group_local(query_two, key_two, value_two, decay_two, DK_B)
    ahead_in = (first[4], first[6], second[4], second[6])
    behind_in = (first[5], first[7], second[5], second[7])
    empty = tuple((jnp.zeros_like(item) for item in ahead_in))
    from_left = carried_in(ahead_in, SP, chain, empty, False)
    from_right = carried_in(behind_in, SP, chain, empty, True)
    mixed_one = (
        first[0]
        + readout(first[2], from_left[1])
        + (first[1] + readout(first[3], from_right[1]))[:, ::-1]
    )
    mixed_two = (
        second[0]
        + readout(second[2], from_left[3])
        + (second[1] + readout(second[3], from_right[3]))[:, ::-1]
    )
    heads_one = finish(mixed_one, gate_one, head_gain)
    heads_two = finish(mixed_two, gate_two, head_gain)
    part = jnp.dot(heads_one, proj_one, preferred_element_type=jnp.float32)
    attn = summed_on_arrival(
        (part + jnp.dot(heads_two, proj_two, preferred_element_type=jnp.float32)).astype(
            jnp.bfloat16
        ),
        "tp",
        0,
    ).astype(jnp.bfloat16)
    stream_own = lax.dynamic_slice_in_dim(stream, tp_rank * own_rows, own_rows, 0)
    settled_own = layer_norm(stream_own.astype(jnp.float32) + attn.astype(jnp.float32), gain_mix)
    moe_in = lax.all_gather(settled_own.astype(jnp.bfloat16), "tp", axis=0, tiled=True)
    top_count = routes.shape[1]
    local_experts = expert_gate.shape[0]
    expert_total = local_experts * sp_count
    capacity = 3 * rows * top_count // (2 * expert_total)
    width = moe_in.shape[1]
    slice_width = width // tp_count
    flat_expert = routes.reshape(-1)
    weights = affinity / jnp.sum(affinity, axis=-1, keepdims=True)
    flat_weights = weights.reshape(-1)
    onehot = (flat_expert[:, None] == jnp.arange(expert_total, dtype=jnp.int32)[None, :]).astype(
        jnp.int32
    )
    rank = jnp.sum(jnp.cumsum(onehot, axis=0) * onehot, axis=1) - 1
    target = flat_expert * capacity + rank
    token = jnp.arange(rows * top_count, dtype=jnp.int32) // top_count
    columns = lax.dynamic_slice_in_dim(moe_in, tp_rank * slice_width, slice_width, 1)
    outgoing = (
        jnp.zeros((expert_total * capacity, slice_width), jnp.bfloat16)
        .at[target]
        .set(columns[token])
    )
    outgoing = outgoing.reshape(sp_count, local_experts, capacity, slice_width)
    arrived = lax.all_to_all(outgoing, SP, split_axis=0, concat_axis=0, tiled=True)
    complete = lax.all_gather(arrived, "tp", axis=3, tiled=True)
    gate = jnp.einsum("secd,edf->secf", complete, expert_gate, preferred_element_type=jnp.float32)
    upward = jnp.einsum("secd,edf->secf", complete, expert_up, preferred_element_type=jnp.float32)
    act = (jax.nn.silu(gate) * upward).astype(jnp.bfloat16)
    partial_value = jnp.einsum(
        "secf,efd->secd", act, expert_down, preferred_element_type=jnp.float32
    ).astype(jnp.bfloat16)
    summed = summed_on_arrival(
        partial_value.astype(jnp.float32).astype(jnp.bfloat16), "tp", 3
    ).astype(jnp.bfloat16)
    returned = lax.all_to_all(summed, SP, split_axis=0, concat_axis=0, tiled=True)
    pieces = returned.reshape(expert_total * capacity, slice_width)[target]
    weighted = pieces.astype(jnp.float32) * flat_weights[:, None]
    term = jnp.sum(weighted.reshape(rows, top_count, slice_width), axis=1)
    mixture = lax.all_to_all(
        term.astype(jnp.bfloat16), "tp", split_axis=0, concat_axis=1, tiled=True
    ).astype(term.dtype)
    return layer_norm(settled_own + mixture, gain_moe).astype(jnp.bfloat16)


def solution(mesh):
    finer = Mesh(mesh.devices.reshape(8, 4, mesh.shape["tp"]), ("sp_0", "sp_1", "tp"))
    return jax.shard_map(
        body,
        mesh=finer,
        in_specs=(
            P(SP, "tp"),
            P(SP, "tp"),
            P(SP, "tp"),
            P(SP, "tp"),
            P(None, SP, "tp"),
            P(SP, "tp"),
            P(SP, "tp"),
            P(SP, "tp"),
            P(SP, "tp"),
            P(None, SP, "tp"),
            P(),
            P("tp", None),
            P("tp", None),
            P(SP, None),
            P(),
            P(),
            P(SP, None),
            P(SP, None),
            P(SP, None, "tp"),
            P(SP, None, "tp"),
            P(SP, "tp", None),
        ),
        out_specs=P(SP_TP, None),
        check_vma=False,
    )
```

profile of v0, /device:TPU:1, one launch (start us, length us, event | category | flops | bytes accessed | tf_op | source)
XLA Modules:
  0.0 402.3 jit_solution(4113022673467742287)
XLA Ops:
  6.6 1.1 fusion.56
  8.8 1.1 fusion.42
  16.2 10.4 %all-gather.4 = bf16[4,194,128]{2,1,0:T(8,128)(2,1)S(1)} all-gather(bf16[1,194,128]{2,1,0:T(8,128)(2,1)S(1)} %maximum_bitcast_fusion), channel_id=2, replica_groups=mesh['sp_0'=8,'sp_1'=4,'tp'=16] {'sp_1'}, dimensions={0}, use_global_device_ids=true | all-gather | bytes 248320 | tf_op jit(solution)/shard_map/all_gather | solution.py:31
  28.1 25.9 %all-gather.5 = bf16[8,194,128]{2,1,0:T(8,128)(2,1)S(1)} all-gather(bf16[1,194,128]{2,1,0:T(8,128)(2,1)S(1)} %maximum_bitcast_fusion.1), channel_id=3, replica_groups=mesh['sp_0'=8,'sp_1'=4,'tp'=16] {'sp_0'}, dimensions={0}, use_global_device_ids=true | all-gather | bytes 446976 | tf_op jit(solution)/shard_map/all_gather | solution.py:31
  58.1 9.6 %all-gather.6 = bf16[4,194,128]{2,1,0:T(8,128)(2,1)S(1)} all-gather(bf16[1,194,128]{2,1,0:T(8,128)(2,1)S(1)} %maximum_bitcast_fusion.2), channel_id=4, replica_groups=mesh['sp_0'=8,'sp_1'=4,'tp'=16] {'sp_1'}, dimensions={0}, use_global_device_ids=true | all-gather | bytes 248320 | tf_op jit(solution)/shard_map/all_gather | solution.py:31
  69.5 19.1 %all-gather.7 = bf16[8,194,128]{2,1,0:T(8,128)(2,1)S(1)} all-gather(bf16[1,194,128]{2,1,0:T(8,128)(2,1)S(1)} %maximum_bitcast_fusion.3), channel_id=5, replica_groups=mesh['sp_0'=8,'sp_1'=4,'tp'=16] {'sp_0'}, dimensions={0}, use_global_device_ids=true | all-gather | bytes 446976 | tf_op jit(solution)/shard_map/all_gather | solution.py:31
  89.4 1.5 reverse.26
  93.1 1.5 convolution_add_fusion.3
  95.6 1.4 multiply_reduce_fusion.2
  99.9 1.4 convolution_add_fusion.7
  102.2 1.4 multiply_reduce_fusion.3
  106.1 1.5 fusion.8
  107.6 25.2 %all-to-all-start = ((bf16[16,16,2048]{2,1,0:T(8,128)(2,1)}), bf16[16,16,2048]{2,1,0:T(8,128)(2,1)S(1)}, u32[]{:S(2)}, u32[]{:S(2)}) async-start(bf16[16,16,2048]{2,1,0:T(8,128)(2,1)} %bitcast.161), calls=%async_computation | async-start | bytes 2097152 | tf_op jit(solution)/shard_map/all_to_all | solution.py:71
  132.8 27.9 %all-to-all-done = bf16[16,16,2048]{2,1,0:T(8,128)(2,1)S(1)} async-done(((bf16[16,16,2048]{2,1,0:T(8,128)(2,1)}), bf16[16,16,2048]{2,1,0:T(8,128)(2,1)S(1)}, u32[]{:S(2)}, u32[]{:S(2)}) %all-to-all-start) | async-done | bytes 1048608 | tf_op jit(solution)/shard_map/all_to_all | solution.py:71
  160.9 1.0 fusion.107
  161.9 1.0 multiply_reduce_fusion.1
  163.0 1.6 fusion.110
  165.3 1.2 reduce-window.46
  167.2 32.0 %all-gather.11.cloned.1.call-done = bf16[256,2048]{1,0:T(8,128)(2,1)} async-done(((bf16[16,2048]{1,0:T(8,128)(2,1)}), bf16[256,2048]{1,0:T(8,128)(2,1)}) %all-gather.11.cloned.1.call-update) | async-done | bytes 1048592 | tf_op jit(solution)/shard_map/all_gather | solution.py:221
  200.1 3.0 scatter_custom_fusion
  203.1 20.4 %all_to_all.30 = bf16[32,1,24,128]{3,2,1,0:T(8,128)(2,1)} all-to-all(bf16[32,1,24,128]{3,2,1,0:T(8,128)(2,1)S(1)} %bitcast.615), channel_id=1, replica_groups=mesh['sp_0'=8,'sp_1'=4,'tp'=16] {'sp_0','sp_1'}, dimensions={0} | all-to-all | bytes 393216 | tf_op jit(solution)/shard_map/all_to_all | solution.py:244
  223.5 42.4 %all-gather.13.cloned.1.call-done = bf16[32,1,24,2048]{3,2,0,1:T(8,128)(2,1)} async-done(((bf16[32,1,24,128]{3,2,0,1:T(8,128)(2,1)}), bf16[32,1,24,2048]{3,2,0,1:T(8,128)(2,1)}) %all-gather.13.cloned.1.call-update) | async-done | bytes 3145744 | tf_op jit(solution)/shard_map/all_gather | solution.py:245
  265.9 2.9 fusion.10
  268.8 6.9 %fusion.9 = bf16[1,32,3,16,8,128]{5,4,3,2,1,0:T(8,128)(2,1)} fusion(bf16[32,1,24,2048]{3,2,0,1:T(8,128)(2,1)} %all-gather.13.cloned.1.call-done, bf16[1,128,2048]{2,1,0:T(8,128)(2,1)S(1)} %copy-done, bf16[1,2048,128]{2,1,0:T(8,128)(2,1)S(1)} %copy-done.6, f32[32,1,24,128]{3,2,0,1:T(8,128)S(1)} %fusion.10), kind=kOutput, calls=%fused_computation.27 | convolution fusion | flops 807469056 | bytes 7733248 | tf_op jit(solution)/shard_map/secf,efd->secd/dot_general | solution.py:249
  275.8 2.7 copy.353
  278.5 77.5 %all_to_all.31 = bf16[16,32,1,24,128]{4,3,1,2,0:T(8,128)(2,1)} all-to-all(bf16[16,32,1,24,128]{4,3,1,2,0:T(8,128)(2,1)S(1)} %bitcast.592), channel_id=1, replica_groups=mesh['sp_0'=8,'sp_1'=4,'tp'=16] {'tp'}, dimensions={0} | all-to-all | bytes 6291456 | tf_op jit(solution)/shard_map/all_to_all | solution.py:71
  356.0 3.1 reduce_sum.113
  359.1 9.9 %all-to-all-start.3 = ((bf16[32,1,24,128]{3,2,1,0:T(8,128)(2,1)}), bf16[32,1,24,128]{3,2,1,0:T(8,128)(2,1)S(1)}, u32[]{:S(2)}, u32[]{:S(2)}) async-start(bf16[32,1,24,128]{3,2,1,0:T(8,128)(2,1)} %bitcast.188), calls=%async_computation.3 | async-start | bytes 393216 | tf_op jit(solution)/shard_map/all_to_all | solution.py:255
  369.2 11.4 %all-to-all-done.3 = bf16[32,1,24,128]{3,2,1,0:T(8,128)(2,1)S(1)} async-done(((bf16[32,1,24,128]{3,2,1,0:T(8,128)(2,1)}), bf16[32,1,24,128]{3,2,1,0:T(8,128)(2,1)S(1)}, u32[]{:S(2)}, u32[]{:S(2)}) %all-to-all-start.3) | async-done | bytes 196640 | tf_op jit(solution)/shard_map/all_to_all | solution.py:255
  380.6 1.3 gather_fusion
  382.4 11.1 %all_to_all.32 = bf16[16,16,128]{2,1,0:T(8,128)(2,1)S(1)} all-to-all(bf16[16,16,128]{2,1,0:T(8,128)(2,1)S(1)} %bitcast.635), channel_id=1, replica_groups=mesh['sp_0'=8,'sp_1'=4,'tp'=16] {'tp'}, dimensions={0} | all-to-all | bytes 131072 | tf_op jit(solution)/shard_map/all_to_all | solution.py:259
  393.4 1.0 fusion.521
  (332 shorter events, 29.5 us)
Async XLA Ops:
  6.5 262.3 %copy-start = (bf16[1,128,2048]{2,1,0:T(8,128)(2,1)S(1)}, bf16[1,128,2048]{2,1,0:T(8,128)(2,1)}, u32[]{:S(2)}) copy-start(bf16[1,128,2048]{2,1,0:T(8,128)(2,1)} %param.49) | copy-start | bytes 1572868
  8.8 48.3 %copy-start.15 = (f32[1,64,2,128]{3,2,0,1:T(2,128)}, f32[1,64,2,128]{3,2,0,1:T(2,128)S(1)}, u32[]{:S(2)}) copy-start(f32[1,64,2,128]{3,2,0,1:T(2,128)S(1)} %copy.288) | copy-start | bytes 196612
  27.8 26.2 %copy-start.24 = (f32[64]{0:T(128)}, f32[64]{0:T(128)S(1)}, u32[]{:S(2)}) copy-start(f32[64]{0:T(128)S(1)} %get-tuple-element.448) | copy-start | bytes 772
  57.1 32.3 %copy-start.17 = (f32[1,64,256]{2,1,0:T(8,128)}, f32[1,64,256]{2,1,0:T(8,128)S(1)}, u32[]{:S(2)}) copy-start(f32[1,64,256]{2,1,0:T(8,128)S(1)} %reshape.2436) | copy-start | bytes 196612
  68.8 26.6 %copy-start.26 = (f32[64]{0:T(128)}, f32[64]{0:T(128)S(1)}, u32[]{:S(2)}) copy-start(f32[64]{0:T(128)S(1)} %get-tuple-element.451) | copy-start | bytes 772
  69.5 26.0 %copy-start.19 = (f32[1,128,256]{1,2,0:T(8,128)S(1)}, f32[1,128,256]{1,2,0:T(8,128)}, u32[]{:S(2)}) copy-start(f32[1,128,256]{1,2,0:T(8,128)} %get-tuple-element.413) | copy-start | bytes 393220
  69.5 26.0 %copy-start.33 = (f32[128]{0:T(128)S(1)}, f32[128]{0:T(128)}, u32[]{:S(2)}) copy-start(f32[128]{0:T(128)} %copy-done.32) | copy-start | bytes 1540
  69.5 26.0 %copy-start.35 = (f32[128]{0:T(128)S(1)}, f32[128]{0:T(128)}, u32[]{:S(2)}) copy-start(f32[128]{0:T(128)} %copy-done.34) | copy-start | bytes 1540
  69.5 26.0 %copy-start.37 = (f32[128]{0:T(128)S(1)}, f32[128]{0:T(128)}, u32[]{:S(2)}) copy-start(f32[128]{0:T(128)} %copy-done.36) | copy-start | bytes 1540
  69.5 26.0 %copy-start.39 = (f32[128]{0:T(128)S(1)}, f32[128]{0:T(128)}, u32[]{:S(2)}) copy-start(f32[128]{0:T(128)} %copy-done.38) | copy-start | bytes 1540
  88.6 6.9 %copy-start.42 = (f32[128]{0:T(128)S(1)}, f32[128]{0:T(128)}, u32[]{:S(2)}) copy-start(f32[128]{0:T(128)} %get-tuple-element.379) | copy-start | bytes 1540
  88.6 6.9 %copy-start.43 = (f32[128]{0:T(128)S(1)}, f32[128]{0:T(128)}, u32[]{:S(2)}) copy-start(f32[128]{0:T(128)} %get-tuple-element.387) | copy-start | bytes 1540
  88.6 6.9 %copy-start.44 = (f32[128]{0:T(128)S(1)}, f32[128]{0:T(128)}, u32[]{:S(2)}) copy-start(f32[128]{0:T(128)} %get-tuple-element.388) | copy-start | bytes 1540
  88.6 6.9 %copy-start.45 = (f32[128]{0:T(128)S(1)}, f32[128]{0:T(128)}, u32[]{:S(2)}) copy-start(f32[128]{0:T(128)} %get-tuple-element.389) | copy-start | bytes 1540
  88.7 6.9 %copy-start.46 = (f32[128]{0:T(128)S(1)}, f32[128]{0:T(128)}, u32[]{:S(2)}) copy-start(f32[128]{0:T(128)} %get-tuple-element.390) | copy-start | bytes 1540
  88.7 6.9 %copy-start.47 = (f32[128]{0:T(128)S(1)}, f32[128]{0:T(128)}, u32[]{:S(2)}) copy-start(f32[128]{0:T(128)} %get-tuple-element.391) | copy-start | bytes 1540
  88.7 6.9 %copy-start.48 = (f32[128]{0:T(128)S(1)}, f32[128]{0:T(128)}, u32[]{:S(2)}) copy-start(f32[128]{0:T(128)} %get-tuple-element.392) | copy-start | bytes 1540
  88.7 6.9 %copy-start.49 = (f32[128]{0:T(128)S(1)}, f32[128]{0:T(128)}, u32[]{:S(2)}) copy-start(f32[128]{0:T(128)} %get-tuple-element.393) | copy-start | bytes 1540
  88.7 6.9 %copy-start.50 = (f32[128]{0:T(128)S(1)}, f32[128]{0:T(128)}, u32[]{:S(2)}) copy-start(f32[128]{0:T(128)} %get-tuple-element.394) | copy-start | bytes 1540
  93.1 6.8 %copy-start.16 = (f32[1,64,2,128]{3,2,0,1:T(2,128)S(1)}, f32[1,64,2,128]{3,2,0,1:T(2,128)}, u32[]{:S(2)}) copy-start(f32[1,64,2,128]{3,2,0,1:T(2,128)} %copy-done.15) | copy-start | bytes 196612
  97.1 8.4 %copy-start.4 = (bf16[128,2048]{1,0:T(8,128)(2,1)S(1)}, bf16[128,2048]{1,0:T(8,128)(2,1)}, u32[]{:S(2)}) copy-start(bf16[128,2048]{1,0:T(8,128)(2,1)} %param.40) | copy-start | bytes 1572868
  97.1 8.4 %copy-start.41 = (f32[128]{0:T(128)S(1)}, f32[128]{0:T(128)}, u32[]{:S(2)}) copy-start(f32[128]{0:T(128)} %param.39) | copy-start | bytes 1540
  106.1 56.9 %copy-start.20 = (f32[2048]{0:T(1024)S(1)}, f32[2048]{0:T(1024)}, u32[]{:S(2)}) copy-start(f32[2048]{0:T(1024)} %param.43) | copy-start | bytes 24580
  106.1 58.8 %copy-start.21 = (s32[256,2]{0,1:T(2,128)S(1)}, s32[256,2]{0,1:T(2,128)}, u32[]{:S(2)}) copy-start(s32[256,2]{0,1:T(2,128)} %param.45) | copy-start | bytes 6148
  107.6 158.3 %copy-start.5 = (bf16[1,2048,128]{2,1,0:T(8,128)(2,1)S(1)}, bf16[1,2048,128]{2,1,0:T(8,128)(2,1)}, u32[]{:S(2)}) copy-start(bf16[1,2048,128]{2,1,0:T(8,128)(2,1)} %param.47) | copy-start | bytes 1572868
  107.6 53.2 %all-to-all-start = ((bf16[16,16,2048]{2,1,0:T(8,128)(2,1)}), bf16[16,16,2048]{2,1,0:T(8,128)(2,1)S(1)}, u32[]{:S(2)}, u32[]{:S(2)}) async-start(bf16[16,16,2048]{2,1,0:T(8,128)(2,1)} %bitcast.161), calls=%async_computation | async-start | bytes 2097152 | tf_op jit(solution)/shard_map/all_to_all | solution.py:71
  132.8 66.4 %all-gather.11.cloned.1.call-start = ((), (), s32[]{:S(2)}) async-start(), calls=%async_computation.5 | async-start | bytes 1114112 | tf_op jit(solution)/shard_map/all_gather | solution.py:221
  163.0 105.9 %copy-start.6 = (bf16[1,2048,128]{2,1,0:T(8,128)(2,1)S(1)}, bf16[1,2048,128]{2,1,0:T(8,128)(2,1)}, u32[]{:S(2)}) copy-start(bf16[1,2048,128]{2,1,0:T(8,128)(2,1)} %param.48) | copy-start | bytes 1572868
  164.6 101.3 %all-gather.13.cloned.1.call-start = ((), (), s32[]{:S(2)}) async-start(), calls=%async_computation.6 | async-start | bytes 3342336 | tf_op jit(solution)/shard_map/all_gather | solution.py:245
  356.0 12.9 %copy-start.23 = (f32[256,2]{0,1:T(2,128)S(1)}, f32[256,2]{0,1:T(2,128)}, u32[]{:S(2)}) copy-start(f32[256,2]{0,1:T(2,128)} %param.46) | copy-start | bytes 6148
  356.0 38.7 %copy-start.22 = (f32[2048]{0:T(1024)S(1)}, f32[2048]{0:T(1024)}, u32[]{:S(2)}) copy-start(f32[2048]{0:T(1024)} %param.44) | copy-start | bytes 24580
  359.1 21.5 %all-to-all-start.3 = ((bf16[32,1,24,128]{3,2,1,0:T(8,128)(2,1)}), bf16[32,1,24,128]{3,2,1,0:T(8,128)(2,1)S(1)}, u32[]{:S(2)}, u32[]{:S(2)}) async-start(bf16[32,1,24,128]{3,2,1,0:T(8,128)(2,1)} %bitcast.188), calls=%async_computation.3 | async-start | bytes 393216 | tf_op jit(solution)/shard_map/all_to_all | solution.py:255
  (30 other events, 101.7 us)
Sparse Core Ops, SparseCore 0:
  164.7 34.4 all-gather.10
  223.7 42.2 all-gather.12
where the time goes:
time: 403 us; the launch traced here: 402 us
  blocking collectives  174 us (43%)
  waiting for transfers between devices  114 us (28%)
  starting transfers between devices  35.3 us (9%)
  other arithmetic  25.8 us (6%)
  matrix products  20.4 us (5%)
  local copies, waits for them, and re-layouts  17.7 us (4%)
  between operations  14.9 us (4%)
    all_to_all x1, blocking collectives, summed_on_arrival(): lax.all_to_all(pieces, axis, split_axis=0, concat_axis=0, tiled=True)  77.5 us
    all_gather x4, blocking collectives, gathered_once(): both, at, found = (lax.all_gather(jnp.concatenate(lines), axis), 0, {})  65 us
    all_gather x1, waiting for transfers between devices, body(): complete = lax.all_gather(arrived, 'tp', axis=3, tiled=True)  42.4 us
    all_gather x1, waiting for transfers between devices, body(): lax.all_gather(settled_own.astype(jnp.bfloat16), 'tp', axis=0, tiled=True)  32 us
    all_to_all x1, waiting for transfers between devices, summed_on_arrival(): lax.all_to_all(pieces, axis, split_axis=0, concat_axis=0, tiled=True)  27.9 us
    all_to_all x1, starting transfers between devices, summed_on_arrival(): lax.all_to_all(pieces, axis, split_axis=0, concat_axis=0, tiled=True)  25.2 us
    all_to_all x1, blocking collectives, body(): lax.all_to_all(outgoing, SP, split_axis=0, concat_axis=0, tiled=True)  20.4 us
    all_to_all x1, waiting for transfers between devices, body(): lax.all_to_all(summed, SP, split_axis=0, concat_axis=0, tiled=True)  11.4 us
  transfers between devices with their start and end apart: 4, of which 4 were waited for; matrix products, arithmetic and copies ran while one was open for 1% of the time, Pallas kernels for 0%

commit v1 on v0

v1 whole, which is shorter than its diff:
```python
import jax
import jax.numpy as jnp
from jax import lax
from jax.experimental import pallas as pl
from jax.experimental.pallas import tpu as pltpu
from jax.sharding import Mesh
from jax.sharding import PartitionSpec as P


DK_A = 64
DK_B = 128
BLK = 64
SHARERS = 4
SLOTS = 6
STEP = 16
SP = ("z", "x")
Y = ("p", "b")
TP = ("p", "b", "c")
ALL = ("z", "x", "p", "b", "c")
SWAP = [(0, 1), (1, 0)]
F32 = jnp.float32
BF16 = jnp.bfloat16
VMEM_LIMIT = 16 * 1024 * 1024
normalizer_sharpness = 16.0


def call(kernel, outs, *args, far=(), scratch=()):
    single = not isinstance(outs, (list, tuple))
    shapes = [outs] if single else list(outs)
    vmem = pl.BlockSpec(memory_space=pltpu.VMEM)
    smem = pl.BlockSpec(memory_space=pltpu.SMEM)
    found = pl.pallas_call(
        kernel,
        out_shape=shapes,
        in_specs=[
            pl.BlockSpec(memory_space=pltpu.HBM)
            if k in far
            else smem
            if arg.ndim == 1
            else vmem
            for k, arg in enumerate(args)
        ],
        out_specs=[vmem] * len(shapes),
        scratch_shapes=list(scratch),
        compiler_params=pltpu.CompilerParams(vmem_limit_bytes=VMEM_LIMIT),
    )(
        *(
            pltpu.with_memory_space_constraint(arg, pltpu.HBM) if k in far else arg
            for k, arg in enumerate(args)
        )
    )
    return found[0] if single else found


def fetched(sources, places, marks):
    copies = [
        pltpu.make_async_copy(source, place, marks.at[k])
        for k, (source, place) in enumerate(zip(sources, places))
    ]
    for copy in copies:
        copy.start()
    return copies


def exact_dot(a, b, dims=((1,), (0,))):
    return lax.dot_general(
        a, b, (dims, ((), ())), precision=lax.Precision.HIGHEST, preferred_element_type=F32
    )


def fast_dot(a, b, dims=((1,), (0,))):
    return lax.dot_general(
        a.astype(BF16), b.astype(BF16), (dims, ((), ())), preferred_element_type=F32
    )


def log_fading(pre):
    return (jnp.minimum(pre, 0.0) - jnp.log1p(jnp.exp(-jnp.abs(pre)))) / normalizer_sharpness


def grid_of(length):
    row = lax.broadcasted_iota(jnp.int32, (length, length), 0)
    col = lax.broadcasted_iota(jnp.int32, (length, length), 1)
    return row, col


def states_kernel(
    d1h, d2h, k1h, v1h, k2h, v2h, gate, up, down, one, two,
    pieces, pack, proj,
    d1, d2, k1, v1, k2, v2, spread, marks, moves,
):
    copies = fetched((d1h, d2h, k1h, v1h, k2h, v2h), (d1, d2, k1, v1, k2, v2), marks)
    features, hidden = gate.shape[1:]
    blocks = down.shape[2] // (2 * hidden)
    sources = [gate.at[0], up.at[0], one, two]
    places = [
        pack.at[:features, :hidden],
        pack.at[:features, hidden:],
        proj.at[:hidden, :],
        proj.at[hidden:, :],
    ]
    for n in range(blocks):
        sources.append(down.at[0, :, 2 * hidden * n : 2 * hidden * (n + 1)])
        places.append(pack.at[features + hidden * n : features + hidden * (n + 1), :])
    moved = fetched(sources, places, moves)
    size, length = k1.shape
    peers = spread.shape[0] // 24
    row, col = grid_of(length)
    above = (row < col).astype(F32)
    below = (row > col).astype(F32)
    ones = jnp.ones((length, 128), F32)

    def put(value, kind, first):
        for n in range(value.shape[0] // peers):
            spread[pl.ds(kind * 6 + first + n, peers, stride=24), :] = value[
                n * peers : (n + 1) * peers
            ]

    copies[0].wait()
    ahead, behind = log_fading(d1[0]), log_fading(d1[1])
    fade_f = jnp.exp(exact_dot(ahead, below))
    fade_b = jnp.exp(exact_dot(behind, above))
    put(exact_dot(ahead, ones), 2, 0)
    put(exact_dot(behind, ones), 3, 0)
    copies[1].wait()
    ahead, behind = log_fading(d2[0]), log_fading(d2[1])
    wide_f = jnp.exp(exact_dot(above, ahead))
    wide_b = jnp.exp(exact_dot(below, behind))
    across = ((0,), (0,))
    put(exact_dot(ahead, ones, across), 2, size // peers)
    put(exact_dot(behind, ones, across), 3, size // peers)
    copies[2].wait()
    copies[3].wait()
    key, value = k1[...].astype(F32), v1[...]
    put(fast_dot(key * fade_f, value), 0, 0)
    put(fast_dot(key * fade_b, value), 1, 0)
    copies[4].wait()
    copies[5].wait()
    key, value = k2[...].astype(F32), v2[...]
    put(fast_dot(key * wide_f, value, across), 0, size // peers)
    put(fast_dot(key * wide_b, value, across), 1, size // peers)
    pieces[...] = spread[...].astype(BF16)
    for copy in moved:
        copy.wait()


def scan_kernel(pieces, out):
    peers, rows2, lanes = pieces.shape
    rows = rows2 // 2
    half = rows // 2
    forward = lax.broadcasted_iota(jnp.int32, (rows, lanes), 0) < half
    state = jnp.zeros((rows, lanes), F32)
    found = []
    for place in range(peers):
        found.append(state)
        if place + 1 < peers:
            whole = pieces[place].astype(F32)
            state = jnp.exp(whole[rows:]) * state + whole[:rows]
    state = jnp.zeros((rows, lanes), F32)
    for place in reversed(range(peers)):
        out[place, :rows] = jnp.where(forward, found[place], state).astype(BF16)
        out[place, rows:] = jnp.zeros((out.shape[1] - rows, lanes), BF16)
        if place > 0:
            whole = pieces[place].astype(F32)
            state = jnp.exp(whole[rows:]) * state + whole[:rows]


def local_kernel(
    q1h, k1h, v1h, d1h, q2h, k2h, v2h, d2h, g1h, g2h, gain,
    mixed, reader_one, reader_two, opened,
    q1, k1, v1, d1, q2, k2, v2, d2, g1, g2, marks,
):
    copies = fetched(
        (q1h, k1h, v1h, d1h, q2h, k2h, v2h, d2h, g1h, g2h),
        (q1, k1, v1, d1, q2, k2, v2, d2, g1, g2),
        marks,
    )
    for copy in copies:
        copy.wait()
    length = v1.shape[0]
    for place, gate in enumerate((g1, g2)):
        value = gate[...].astype(F32)
        opened[:, place * 128 : (place + 1) * 128] = value * jax.nn.sigmoid(value) * gain[...]
    count = length // BLK
    row, col = grid_of(length)
    upto = (col <= row).astype(F32)
    since = (col >= row).astype(F32)
    brow, bcol = grid_of(BLK)
    lower, upper = bcol <= brow, bcol >= brow
    on_last = ((1,), (1,))
    at = 0
    for q_ref, k_ref, v_ref, d_ref, reader in (
        (q1, k1, v1, d1, reader_one),
        (q2, k2, v2, d2, reader_two),
    ):
        size = reader.shape[1] // 2
        query = q_ref[...].astype(F32) * size ** (-0.5)
        key = k_ref[...].astype(F32)
        value = v_ref[...]
        ahead, behind = d_ref[0], d_ref[1]
        if size == DK_A:
            query, key, ahead, behind = query.T, key.T, ahead.T, behind.T
        ahead, behind = log_fading(ahead), log_fading(behind)
        cum_f = exact_dot(upto, ahead)
        cum_b = exact_dot(since, behind)
        reader[:, :size] = (query * jnp.exp(cum_f)).astype(BF16)
        reader[:, size:] = (query * jnp.exp(cum_b)).astype(BF16)
        sums = []
        for i in range(count):
            part = slice(i * BLK, (i + 1) * BLK)
            own_f, own_b = ahead[part], behind[part]
            local_f = exact_dot(upto[:BLK, :BLK], own_f)
            local_b = exact_dot(since[:BLK, :BLK], own_b)
            q_i, k_i = query[part], key[part]
            score_f = fast_dot(q_i * jnp.exp(local_f), k_i * jnp.exp(-local_f), on_last)
            score_b = fast_dot(q_i * jnp.exp(local_b), k_i * jnp.exp(-local_b), on_last)
            score = jnp.where(lower, score_f, 0.0) + jnp.where(upper, score_b, 0.0)
            sums.append(fast_dot(score, value[part]))
        for j in range(count):
            part = slice(j * BLK, (j + 1) * BLK)
            if j + 1 < count:
                rest = slice((j + 1) * BLK, length)
                end = cum_f[(j + 1) * BLK - 1 : (j + 1) * BLK]
                gone = fast_dot(
                    query[rest] * jnp.exp(cum_f[rest] - end),
                    key[part] * jnp.exp(end - cum_f[part]),
                    on_last,
                )
                carried = fast_dot(gone, value[part])
                for i in range(j + 1, count):
                    sums[i] = sums[i] + carried[(i - j - 1) * BLK : (i - j) * BLK]
            if j > 0:
                rest = slice(0, j * BLK)
                end = cum_b[j * BLK : j * BLK + 1]
                gone = fast_dot(
                    query[rest] * jnp.exp(cum_b[rest] - end),
                    key[part] * jnp.exp(end - cum_b[part]),
                    on_last,
                )
                carried = fast_dot(gone, value[part])
                for i in range(j):
                    sums[i] = sums[i] + carried[i * BLK : (i + 1) * BLK]
        for i in range(count):
            mixed[i * BLK : (i + 1) * BLK, at : at + 128] = sums[i]
        at += 128


def heads_kernel(
    core, local, reader_one, reader_two, carried, opened, own, sent, both, spread
):
    width = 128
    length = local.shape[0]
    spread[...] = carried[...].astype(F32)
    peers = spread.shape[0] // 16

    def state(first, last):
        return jnp.concatenate(
            [
                spread[pl.ds(kind * 6 + n, peers, stride=16), :]
                for kind in range(2)
                for n in range(first, last)
            ],
            axis=0,
        )

    at = 0
    for reader, held in ((reader_one, state(0, 2)), (reader_two, state(2, 6))):
        mixed = local[:, at : at + width] + fast_dot(reader[...], held)
        scale = lax.rsqrt(jnp.mean(mixed * mixed, axis=-1, keepdims=True) + 1e-06)
        heads = (mixed * scale * opened[:, at : at + width]).astype(BF16)
        for turn in range(length // STEP):
            where = (turn // 2) * STEP
            both[turn % 2, where : where + STEP, at : at + width] = heads[
                turn * STEP : (turn + 1) * STEP
            ]
        at += width
    own[...] = both[core[0]]
    sent[...] = both[1 - core[0]]


def routing_kernel(where, routes, affinity, chosen, weighted):
    core, first = where[0], where[1]
    rows = routes.shape[1]
    slots = chosen.shape[0]
    experts = slots // SLOTS
    half = rows // 2
    row, col = grid_of(rows)
    inner = lax.rem(row, half)
    turn = jnp.where(row < half, core, 1 - core)
    token = 2 * STEP * lax.div(inner, STEP) + STEP * turn + lax.rem(inner, STEP)
    order = (token == col).astype(F32)
    lane = lax.broadcasted_iota(jnp.int32, (experts, rows), 0)
    named = [routes[k : k + 1, :] for k in range(2)]
    hot = [(lane == name).astype(F32) for name in named]
    before = fast_dot(hot[0] + hot[1], (row < col).astype(BF16))
    share = affinity[...]
    share = share / jnp.sum(share, axis=0, keepdims=True)
    lines = []
    for k in range(2):
        rank = jnp.sum(hot[k] * before, axis=0, keepdims=True).astype(jnp.int32) - first
        inside = (rank >= 0) & (rank < SLOTS)
        spot = jnp.where(inside, rank * experts + named[k], -1)
        lines.append(spot.astype(F32))
    lines += [share[0:1, :], share[1:2, :]]
    lines = jnp.concatenate(lines + [jnp.zeros((4, rows), F32)], axis=0)
    flat = exact_dot(lines, order, ((1,), (1,)))
    tall = exact_dot(order, lines, ((1,), (1,)))
    place = lax.broadcasted_iota(jnp.int32, (slots, rows), 0).astype(F32)
    hit = (place == flat[0:1, :]) | (place == flat[1:2, :])
    chosen[...] = hit.astype(F32).astype(BF16)
    place = lax.broadcasted_iota(jnp.int32, (rows, slots), 1).astype(F32)
    scaled = jnp.where(place == tall[:, 0:1], tall[:, 2:3], 0.0)
    scaled = scaled + jnp.where(place == tall[:, 1:2], tall[:, 3:4], 0.0)
    weighted[...] = scaled.astype(BF16)


def loosen(packed, spread):
    for n in range(spread.shape[0]):
        spread[n] = packed[:, n * 128 : (n + 1) * 128].astype(F32)


def tighten(spread, packed):
    for n in range(spread.shape[0]):
        packed[:, n * 128 : (n + 1) * 128] = spread[n].astype(BF16)


def strided(part, slot, peers):
    return pl.ds(part * SLOTS + slot, peers, stride=SHARERS * SLOTS)


def taken(spread, part):
    peers = spread.shape[1] // (SHARERS * SLOTS)
    return jnp.concatenate(
        [
            jnp.concatenate(
                [spread[n, strided(part, slot, peers), :] for slot in range(SLOTS)], axis=0
            ).astype(BF16)
            for n in range(spread.shape[0])
        ],
        axis=1,
    )


def placed(spread, part, value, lane):
    peers = spread.shape[1] // (SHARERS * SLOTS)
    for n in range(value.shape[1] // 128):
        for slot in range(SLOTS):
            spread[lane + n, strided(part, slot, peers), :] = value[
                slot * peers : (slot + 1) * peers, n * 128 : (n + 1) * 128
            ]


def dispatch_kernel(chosen, own, other, out, spread):
    wide = out.shape[1]
    for part in range(SHARERS):
        lanes = slice(part * wide, (part + 1) * wide)
        both = jnp.concatenate([own[:, lanes], other[:, lanes]], axis=0)
        placed(spread, part, fast_dot(chosen[...], both), 0)
    tighten(spread, out)


def expert_kernel(rows, own, near, side, far, out, spread):
    wide = rows.shape[1]
    hidden = own.shape[1] // 2
    packs = (own, near, side, far)
    loosen(rows, spread)
    x = jnp.concatenate([taken(spread, part) for part in range(SHARERS)], axis=1)
    features = SHARERS * wide
    acts = []
    for pack in packs:
        both = fast_dot(x, pack[:features, :])
        gate, upward = both[:, :hidden], both[:, hidden:]
        acts.append((gate * jax.nn.sigmoid(gate) * upward).astype(BF16))
    acts = [jnp.concatenate(acts[:2], axis=1), jnp.concatenate(acts[2:], axis=1)]
    step = 2 * hidden
    for n in range(features // step):
        here = slice(features + n * hidden, features + (n + 1) * hidden)
        value = 0.0
        for act, pair in zip(acts, (packs[:2], packs[2:])):
            value = value + fast_dot(act, jnp.concatenate([pack[here, :] for pack in pair], axis=0))
        placed(spread, n * step // wide, value, n * step % wide // 128)
    tighten(spread, out)


def combine_kernel(weighted, returned, own, sent, spread):
    half = own.shape[0]
    wide = returned.shape[1]
    loosen(returned, spread)
    for part in range(SHARERS):
        value = fast_dot(weighted[...], taken(spread, part))
        own[:, part * wide : (part + 1) * wide] = value[:half]
        sent[:, part * wide : (part + 1) * wide] = value[half:].astype(BF16)


def settle_kernel(parts, stream, gain, settled, copies):
    total = 0.0
    for place in range(parts.shape[0]):
        total = total + parts[place].astype(F32)
    attn = total.astype(BF16).astype(F32)
    found = layer_norm(stream[...].astype(F32) + attn, gain[...])
    settled[...] = found
    for place in range(parts.shape[0]):
        copies[place] = found.astype(BF16)


def finish_kernel(parts, settled, gain, out):
    total = 0.0
    for place in range(parts.shape[0]):
        total = total + parts[place].astype(F32)
    out[...] = layer_norm(settled[...] + total, gain[...]).astype(BF16)


def join_kernel(own, got, out):
    out[...] = (own[...] + got[...].astype(F32)).astype(BF16)


def project_kernel(own, got, proj, other, out):
    width = out.shape[1]
    step = width // 4
    for n in range(4):
        lanes = slice(n * step, (n + 1) * step)
        value = fast_dot(own[...], proj[:, lanes]) + fast_dot(got[...], other[:, lanes])
        out[:, lanes] = value.astype(BF16)


def layer_norm(values, gain):
    mean = jnp.mean(values, axis=-1, keepdims=True)
    spread = jnp.mean(jnp.square(values - mean), axis=-1, keepdims=True)
    return (values - mean) * lax.rsqrt(spread + 1e-05) * gain


def exchange(pieces, axis):
    return lax.all_to_all(pieces, axis, split_axis=0, concat_axis=0, tiled=True)


def swapped(value, axis):
    return lax.ppermute(value, axis, SWAP)


def tied(value, after):
    return lax.optimization_barrier((value, after))[0]


def body(
    query_one,
    key_one,
    value_one,
    gate_one,
    decay_one,
    query_two,
    key_two,
    value_two,
    gate_two,
    decay_two,
    head_gain,
    proj_one,
    proj_two,
    stream,
    gain_mix,
    gain_moe,
    routes,
    affinity,
    expert_gate,
    expert_up,
    expert_down,
):
    return layer(
        query_one.T,
        key_one.T,
        value_one,
        gate_one,
        jnp.swapaxes(decay_one, 1, 2),
        query_two,
        key_two,
        value_two,
        gate_two,
        decay_two,
        head_gain,
        proj_one,
        proj_two,
        stream,
        gain_mix,
        gain_moe,
        routes,
        affinity,
        expert_gate,
        expert_up,
        expert_down,
    )


def layer(
    query_one,
    key_one,
    value_one,
    gate_one,
    decay_one,
    query_two,
    key_two,
    value_two,
    gate_two,
    decay_two,
    head_gain,
    proj_one,
    proj_two,
    stream,
    gain_mix,
    gain_moe,
    routes,
    affinity,
    expert_gate,
    expert_up,
    expert_down,
):
    rows = query_two.shape[0]
    width = stream.shape[1]
    peers = lax.axis_size(SP)
    chips = lax.axis_size(Y)
    tp_count = lax.axis_size(TP)
    own_rows = rows // tp_count
    half = rows // 2
    core = lax.axis_index("c")
    tp_rank = lax.axis_index(TP)
    group = lax.axis_index(("b", "c"))
    hidden = expert_gate.shape[2]
    slots = peers * SLOTS
    total = SHARERS * slots
    wide = width // SHARERS
    keys = DK_A + DK_B
    shape = jax.ShapeDtypeStruct

    def scratch(items):
        held = [pltpu.VMEM(item.shape, item.dtype) for item in items]
        return held, pltpu.SemaphoreType.DMA((len(items),))

    early = (decay_one, decay_two, key_one, value_one, key_two, value_two)
    moves = (expert_gate, expert_up, expert_down, proj_one, proj_two)
    held, marks = scratch(early)
    lines = 4 * keys
    blocks = width // (2 * hidden)
    pieces, pack, proj = call(
        states_kernel,
        [
            pltpu.HBM((lines, 128), BF16),
            shape((width + blocks * hidden, 2 * hidden), BF16),
            shape((2 * hidden, width), BF16),
        ],
        *early,
        *moves,
        far=range(len(early) + len(moves)),
        scratch=held
        + [pltpu.VMEM((lines, 128), F32), marks, pltpu.SemaphoreType.DMA((4 + blocks,))],
    )
    pieces = pieces.reshape(peers, lines // peers, 128)
    near = swapped(pack, "b")
    side = swapped(pack, "c")
    proj_other = swapped(proj, "c")
    arrived = exchange(pieces, SP)
    late = (
        query_one,
        key_one,
        value_one,
        decay_one,
        query_two,
        key_two,
        value_two,
        decay_two,
        gate_one,
        gate_two,
    )
    held, marks = scratch(late)
    local, reader_one, reader_two, opened = call(
        local_kernel,
        [
            shape((rows, 256), F32),
            shape((rows, 2 * DK_A), BF16),
            shape((rows, 2 * DK_B), BF16),
            shape((rows, 256), F32),
        ],
        *late,
        head_gain.reshape(1, 128),
        far=range(len(late)),
        scratch=held + [marks],
    )
    chosen, weighted = call(
        routing_kernel,
        [shape((slots, rows), BF16), shape((rows, slots), BF16)],
        jnp.stack([core, group * SLOTS]).astype(jnp.int32),
        routes.T,
        affinity.T,
    )
    starts = call(
        scan_kernel, pltpu.HBM((peers, 16, 128), BF16), arrived
    )
    carried = exchange(starts, SP).reshape(peers * 16, 128)
    heads_own, heads_sent = call(
        heads_kernel,
        [shape((half, 256), BF16)] * 2,
        core.reshape(1).astype(jnp.int32),
        local,
        reader_one,
        reader_two,
        carried,
        opened,
        scratch=[pltpu.VMEM((2, half, 256), BF16), pltpu.VMEM((peers * 16, 128), F32)],
    )
    far = swapped(tied(near, heads_own), "c")
    heads_got = swapped(heads_sent, "c")
    part = call(
        project_kernel, pltpu.HBM((half, width), BF16), heads_own, heads_got, proj, proj_other
    )
    attn = exchange(part.reshape(chips, own_rows, width), Y)
    stream_own = lax.dynamic_slice_in_dim(stream, tp_rank * own_rows, own_rows, 0)
    settled, mine = call(
        settle_kernel,
        [shape((own_rows, width), F32), pltpu.HBM((chips, own_rows, width), BF16)],
        attn,
        stream_own,
        gain_mix.reshape(1, width),
    )
    moe_own = exchange(mine, Y).reshape(half, width)
    moe_other = swapped(moe_own, "c")
    spread = [pltpu.VMEM((wide // 128, total, 128), F32)]
    outgoing = call(
        dispatch_kernel,
        pltpu.HBM((total, wide), BF16),
        chosen,
        moe_own,
        moe_other,
        scratch=spread,
    )
    complete = exchange(outgoing.reshape(peers, total // peers, wide), SP)
    partial = call(
        expert_kernel,
        pltpu.HBM((total, wide), BF16),
        complete.reshape(total, wide),
        pack,
        near,
        side,
        far,
        scratch=spread,
    )
    returned = exchange(partial.reshape(peers, total // peers, wide), SP)
    term_own, term_sent = call(
        combine_kernel,
        [shape((half, width), F32), shape((half, width), BF16)],
        weighted,
        returned.reshape(total, wide),
        scratch=spread,
    )
    term = call(join_kernel, pltpu.HBM((half, width), BF16), term_own, swapped(term_sent, "c"))
    mixture = exchange(term.reshape(chips, own_rows, width), Y)
    return call(
        finish_kernel,
        shape((own_rows, width), BF16),
        mixture,
        settled,
        gain_moe.reshape(1, width),
    )


def solution(mesh):
    finer = Mesh(mesh.devices.reshape(8, 4, 4, 2, 2), ALL)
    return jax.shard_map(
        body,
        mesh=finer,
        in_specs=(
            P(SP, TP),
            P(SP, TP),
            P(SP, TP),
            P(SP, TP),
            P(None, SP, TP),
            P(SP, TP),
            P(SP, TP),
            P(SP, TP),
            P(SP, TP),
            P(None, SP, TP),
            P(),
            P(TP, None),
            P(TP, None),
            P(SP, None),
            P(),
            P(),
            P(SP, None),
            P(SP, None),
            P(SP, None, TP),
            P(SP, None, TP),
            P(SP, TP, None),
        ),
        out_specs=P(ALL, None),
        check_vma=False,
    )
```

time: 403 us -> 224 us (0.56)
  waiting for transfers between devices: 114 us -> 43.7 us
  blocking collectives: 174 us -> 110 us
  Pallas kernels: 0 us -> 26.2 us
  other arithmetic: 25.8 us -> 0.08 us
  matrix products: 20.4 us -> 0 us
  local copies, waits for them, and re-layouts: 17.7 us -> 0.04 us
  between operations: 14.9 us -> 0.2 us
  starting transfers between devices: 35.3 us -> 43.4 us
    all_gather x2 -> x0, waiting for transfers between devices: 74.4 us -> none  [the longest x1 42.4 us: body(): complete = lax.all_gather(arrived, 'tp', axis=3, tiled=True)]
    all_gather x4 -> x0, blocking collectives: 65 us -> none  [gathered_once(): both, at, found = (lax.all_gather(jnp.concatenate(lines), axis), 0, {})]
    ppermute x0 -> x7, starting transfers between devices: none -> 28.4 us  [swapped(): return lax.ppermute(value, axis, SWAP)]
    pallas_call x0 -> x12, Pallas kernels: none -> 26.2 us  [call(): pl.pallas_call(kernel, out_shape=shapes, in_specs=[pl.BlockSpec(memory_sp...]
    dot_general x20 -> x0, matrix products: 20.4 us -> none  [the longest x1 6.95 us: body(): jnp.einsum('secf,efd->secd', act, expert_down, preferred_element_type=jnp...]
    all_to_all x2 -> x3, starting transfers between devices: 35.1 us -> 15 us  [exchange(): return lax.all_to_all(pieces, axis, split_axis=0, concat_axis=0, tiled=True)]
    reduce_sum x9 -> x0, other arithmetic: 7.02 us -> none  [the longest x2 3.2 us: summed_on_arrival(): return arrived.astype(jnp.float32).sum(axis=0)]
    another operation x18 -> x1, other arithmetic: 4.84 us -> 0.08 us  [layer(): jnp.stack([core, group * SLOTS]).astype(jnp.int32)]
  transfers between devices with their start and end apart: 4 -> 10, of which waited for: 4 -> 5; matrix products, arithmetic and copies ran while one was open for 1% -> 0% of each run, Pallas kernels for 0% -> 5%
where the time goes in v1:
time: 224 us
  blocking collectives  110 us (49%)
  waiting for transfers between devices  43.7 us (20%)
  starting transfers between devices  43.4 us (19%)
  Pallas kernels  26.2 us (12%)
    all_to_all x4, blocking collectives, exchange(): return lax.all_to_all(pieces, axis, split_axis=0, concat_axis=0, tiled=True)  110 us
    all_to_all x3, waiting for transfers between devices, exchange(): return lax.all_to_all(pieces, axis, split_axis=0, concat_axis=0, tiled=True)  41.3 us
    ppermute x7, starting transfers between devices, swapped(): return lax.ppermute(value, axis, SWAP)  28.4 us
    pallas_call x12, Pallas kernels, call(): pl.pallas_call(kernel, out_shape=shapes, in_specs=[pl.BlockSpec(memory_sp...  26.2 us
    all_to_all x3, starting transfers between devices, exchange(): return lax.all_to_all(pieces, axis, split_axis=0, concat_axis=0, tiled=True)  15 us
  transfers between devices with their start and end apart: 10, of which 5 were waited for; matrix products, arithmetic and copies ran while one was open for 0% of the time, Pallas kernels for 5%

profile of v1, /device:TPU:1, one launch (start us, length us, event | category | flops | bytes accessed | tf_op | source)
XLA Modules:
  0.0 223.5 jit_solution(7609946971143376434)
XLA Ops:
  0.0 4.9 %shard_map.201 = (bf16[768,128]{1,0:T(8,128)(2,1)}, bf16[3072,256]{1,0:T(8,128)(2,1)S(1)}, bf16[256,2048]{1,0:T(8,128)(2,1)}) custom-call(f32[2,64,256]{2,1,0:T(8,128)} %bitcast.33, f32[2,256,128]{2,1,0:T(8,128)} %d2h.3, bf16[64,256]{1,0:T(8,128)(2,1)} %bitcast.36, bf16[256,128]{1,0:T(8,128)(2,1)} %v1h.3, bf16[256,128]{1,0:T(8,128)(2,1)} %k2h.3, ...), custom_call_target="tpu_custom_call" | custom-call | tf_op jit(solution)/shard_map/pallas_call | solution.py:32
  4.9 8.7 %collective-permute-start.1 = (bf16[256,2048]{1,0:T(8,128)(2,1)}, bf16[256,2048]{1,0:T(8,128)(2,1)}, u32[]{:S(2)}, u32[]{:S(2)}) collective-permute-start(bf16[256,2048]{1,0:T(8,128)(2,1)} %get-tuple-element.30.proj), channel_id=1, source_target_pairs={{0,1},{1,0},{2,3},{3,2},{4,5},{5,4},{6,7},{7,6},{8,9},{9,8},{10,11... | collective-permute-start | bytes 3145736 | tf_op jit(solution)/shard_map/ppermute | solution.py:437
  13.6 18.2 %all_to_all.35.pieces = bf16[32,24,128]{2,1,0:T(8,128)(2,1)S(1)} all-to-all(bf16[32,24,128]{2,1,0:T(8,128)(2,1)} %bitcast.35), channel_id=1, replica_groups=mesh['z'=8,'x'=4,'p'=4,'b'=2,'c'=2] {'z','x'}, dimensions={0} | all-to-all | bytes 393216 | tf_op jit(solution)/shard_map/all_to_all | solution.py:433
  31.9 0.8 shard_map.202
  32.7 4.1 %all-to-all-start.1 = ((bf16[32,16,128]{2,1,0:T(8,128)(2,1)}), bf16[32,16,128]{2,1,0:T(8,128)(2,1)S(1)}, u32[]{:S(2)}, u32[]{:S(2)}) async-start(bf16[32,16,128]{2,1,0:T(8,128)(2,1)} %shard_map.202), calls=%async_computation.1 | async-start | bytes 262144 | tf_op jit(solution)/shard_map/all_to_all | solution.py:433
  36.8 4.7 %shard_map.200 = (f32[256,256]{1,0:T(8,128)S(1)}, bf16[256,128]{1,0:T(8,128)(2,1)S(1)}, bf16[256,256]{1,0:T(8,128)(2,1)S(1)}, f32[256,256]{1,0:T(8,128)S(1)}) custom-call(bf16[64,256]{1,0:T(8,128)(2,1)} %bitcast.38, bf16[64,256]{1,0:T(8,128)(2,1)} %bitcast.37, bf16[256,128]{1,0:T(8,128)(2,1)} %v1h.3, f32[2,64,256]{2,1,0:T(8,128)} %bitcast.34, ...), custom_call_target="tpu_custom_call" | custom-call | tf_op jit(solution)/shard_map/pallas_call | solution.py:32
  41.6 4.6 %all-to-all-done.1 = bf16[32,16,128]{2,1,0:T(8,128)(2,1)S(1)} async-done(((bf16[32,16,128]{2,1,0:T(8,128)(2,1)}), bf16[32,16,128]{2,1,0:T(8,128)(2,1)S(1)}, u32[]{:S(2)}, u32[]{:S(2)}) %all-to-all-start.1) | async-done | bytes 131104 | tf_op jit(solution)/shard_map/all_to_all | solution.py:433
  46.2 0.4 shard_map.203
  46.6 4.8 %collective-permute-start = (bf16[128,256]{1,0:T(8,128)(2,1)S(1)}, bf16[128,256]{1,0:T(8,128)(2,1)S(1)}, u32[]{:S(2)}, u32[]{:S(2)}) collective-permute-start(bf16[128,256]{1,0:T(8,128)(2,1)S(1)} %get-tuple-element.29), channel_id=1, source_target_pairs={{0,1},{1,0},{2,3},{3,2},{4,5},{5,4},{6,7},{7,6},{8,9},{9,8},{10,11... | collective-permute-start | bytes 196616 | tf_op jit(solution)/shard_map/ppermute | solution.py:437
  51.3 0.9 collective-permute-done.got
  52.2 2.8 %shard_map.204 = bf16[128,2048]{1,0:T(8,128)(2,1)} custom-call(bf16[128,256]{1,0:T(8,128)(2,1)S(1)} %get-tuple-element.28.own, bf16[128,256]{1,0:T(8,128)(2,1)S(1)} %collective-permute-done.got, bf16[256,2048]{1,0:T(8,128)(2,1)} %get-tuple-element.30.proj, bf16[256,2048]{1,0:T(8,128)(2,1)} %collective-permute-done.1.other), custom_call_target="tpu_custom_call" | custom-call | tf_op jit(solution)/shard_map/pallas_call | solution.py:32
  55.0 6.9 %all-to-all-start.2 = ((bf16[8,16,2048]{2,1,0:T(8,128)(2,1)}), bf16[8,16,2048]{2,1,0:T(8,128)(2,1)S(1)}, u32[]{:S(2)}, u32[]{:S(2)}) async-start(bf16[8,16,2048]{2,1,0:T(8,128)(2,1)} %bitcast.31), calls=%async_computation.2 | async-start | bytes 1048576 | tf_op jit(solution)/shard_map/all_to_all | solution.py:433
  62.0 3.4 %collective-permute-start.3 = (bf16[3072,256]{1,0:T(8,128)(2,1)S(1)}, bf16[3072,256]{1,0:T(8,128)(2,1)}, u32[]{:S(2)}, u32[]{:S(2)}) collective-permute-start(bf16[3072,256]{1,0:T(8,128)(2,1)S(1)} %get-tuple-element.32.own), channel_id=1, source_target_pairs={{0,2},{2,0},{1,3},{3,1},{4,6},{6,4},{5,7},{7,5},{8,10},{10,8},{9,1... | collective-permute-start | bytes 4718600 | tf_op jit(solution)/shard_map/ppermute | solution.py:437
  65.4 14.4 %all-to-all-done.2.parts = bf16[8,16,2048]{2,1,0:T(8,128)(2,1)S(1)} async-done(((bf16[8,16,2048]{2,1,0:T(8,128)(2,1)}), bf16[8,16,2048]{2,1,0:T(8,128)(2,1)S(1)}, u32[]{:S(2)}, u32[]{:S(2)}) %all-to-all-start.2) | async-done | bytes 524320 | tf_op jit(solution)/shard_map/all_to_all | solution.py:433
  79.8 1.1 shard_map.205
  80.9 44.0 %all_to_all.36 = bf16[8,16,2048]{2,1,0:T(8,128)(2,1)S(1)} all-to-all(bf16[8,16,2048]{2,1,0:T(8,128)(2,1)} %get-tuple-element.31), channel_id=1, replica_groups=mesh['z'=8,'x'=4,'p'=4,'b'=2,'c'=2] {'p','b'}, dimensions={0} | all-to-all | bytes 1048576 | tf_op jit(solution)/shard_map/all_to_all | solution.py:433
  124.9 2.4 %collective-permute-start.2 = (bf16[128,2048]{1,0:T(8,128)(2,1)S(1)}, bf16[128,2048]{1,0:T(8,128)(2,1)}, u32[]{:S(2)}, u32[]{:S(2)}) collective-permute-start(bf16[128,2048]{1,0:T(8,128)(2,1)S(1)} %bitcast.21), channel_id=1, source_target_pairs={{0,1},{1,0},{2,3},{3,2},{4,5},{5,4},{6,7},{7,6},{8,9},{9,8},{10,11... | collective-permute-start | bytes 1572872 | tf_op jit(solution)/shard_map/ppermute | solution.py:437
  127.3 1.9 collective-permute-start.4
  129.2 2.4 %collective-permute-start.5 = (bf16[3072,256]{1,0:T(8,128)(2,1)}, bf16[3072,256]{1,0:T(8,128)(2,1)}, u32[]{:S(2)}, u32[]{:S(2)}) collective-permute-start(bf16[3072,256]{1,0:T(8,128)(2,1)} %collective-permute-done.3.near), channel_id=1, source_target_pairs={{0,1},{1,0},{2,3},{3,2},{4,5},{5,4},{6,7},{7,6},{8,9},{9,8},{10,11... | collective-permute-start | bytes 4718600 | tf_op jit(solution)/shard_map/ppermute | solution.py:437
  131.6 0.1 pad_add_fusion.where
  131.7 1.4 shard_map.199
  133.1 2.7 %shard_map.206 = bf16[768,512]{1,0:T(8,128)(2,1)} custom-call(bf16[192,256]{1,0:T(8,128)(2,1)S(1)} %get-tuple-element.22.chosen, bf16[128,2048]{1,0:T(8,128)(2,1)S(1)} %bitcast.22, bf16[128,2048]{1,0:T(8,128)(2,1)} %collective-permute-done.2.other), custom_call_target="tpu_custom_call" | custom-call | tf_op jit(solution)/shard_map/pallas_call | solution.py:32
  135.8 3.9 %all-to-all-start.4 = ((bf16[32,24,512]{2,1,0:T(8,128)(2,1)}), bf16[32,24,512]{2,1,0:T(8,128)(2,1)S(1)}, u32[]{:S(2)}, u32[]{:S(2)}) async-start(bf16[32,24,512]{2,1,0:T(8,128)(2,1)} %bitcast.29), calls=%async_computation.4 | async-start | bytes 1572864 | tf_op jit(solution)/shard_map/all_to_all | solution.py:433
  139.7 22.3 %all-to-all-done.4 = bf16[32,24,512]{2,1,0:T(8,128)(2,1)S(1)} async-done(((bf16[32,24,512]{2,1,0:T(8,128)(2,1)}), bf16[32,24,512]{2,1,0:T(8,128)(2,1)S(1)}, u32[]{:S(2)}, u32[]{:S(2)}) %all-to-all-start.4) | async-done | bytes 786464 | tf_op jit(solution)/shard_map/all_to_all | solution.py:433
  162.0 5.1 %shard_map.207 = bf16[768,512]{1,0:T(8,128)(2,1)} custom-call(bf16[768,512]{1,0:T(8,128)(2,1)S(1)} %bitcast.20, bf16[3072,256]{1,0:T(8,128)(2,1)S(1)} %get-tuple-element.32.own, bf16[3072,256]{1,0:T(8,128)(2,1)} %collective-permute-done.3.near, bf16[3072,256]{1,0:T(8,128)(2,1)} %collective-permute-done.4.side, bf16[3072,256]{1,0:T(8,128)(2,1)} %collective-permute-done.5.far), custom_call_target="tpu_custom_call" | custom-call | tf_op jit(solution)/shard_map/pallas_call | solution.py:32
  167.1 26.4 %all_to_all.37 = bf16[32,24,512]{2,1,0:T(8,128)(2,1)S(1)} all-to-all(bf16[32,24,512]{2,1,0:T(8,128)(2,1)} %bitcast.30), channel_id=1, replica_groups=mesh['z'=8,'x'=4,'p'=4,'b'=2,'c'=2] {'z','x'}, dimensions={0} | all-to-all | bytes 1572864 | tf_op jit(solution)/shard_map/all_to_all | solution.py:433
  193.5 0.6 shard_map.208
  194.1 4.8 %collective-permute-start.6 = (bf16[128,2048]{1,0:T(8,128)(2,1)S(1)}, bf16[128,2048]{1,0:T(8,128)(2,1)S(1)}, u32[]{:S(2)}, u32[]{:S(2)}) collective-permute-start(bf16[128,2048]{1,0:T(8,128)(2,1)S(1)} %get-tuple-element.35), channel_id=1, source_target_pairs={{0,1},{1,0},{2,3},{3,2},{4,5},{5,4},{6,7},{7,6},{8,9},{9,8},{10,11... | collective-permute-start | bytes 1572872 | tf_op jit(solution)/shard_map/ppermute | solution.py:437
  198.9 1.5 collective-permute-done.6.got
  200.4 0.9 shard_map.209
  201.3 21.3 %all_to_all.38.parts = bf16[8,16,2048]{2,1,0:T(8,128)(2,1)S(1)} all-to-all(bf16[8,16,2048]{2,1,0:T(8,128)(2,1)} %bitcast.32), channel_id=1, replica_groups=mesh['z'=8,'x'=4,'p'=4,'b'=2,'c'=2] {'p','b'}, dimensions={0} | all-to-all | bytes 1048576 | tf_op jit(solution)/shard_map/all_to_all | solution.py:433
  222.6 0.9 shard_map.210
  (22 shorter events, 0.1 us)
Async XLA Ops:
  0.0 65.4 %copy-start = (bf16[256,2048]{1,0:T(8,128)(2,1)S(1)}, bf16[256,2048]{1,0:T(8,128)(2,1)}, u32[]{:S(2)}) copy-start(bf16[256,2048]{1,0:T(8,128)(2,1)} %param.34) | copy-start | bytes 3145732
  0.0 36.8 %copy-start.7 = (f32[128]{0:T(128)S(1)}, f32[128]{0:T(128)}, u32[]{:S(2)}) copy-start(f32[128]{0:T(128)} %param.31) | copy-start | bytes 1540
  4.9 47.3 %collective-permute-start.1 = (bf16[256,2048]{1,0:T(8,128)(2,1)}, bf16[256,2048]{1,0:T(8,128)(2,1)}, u32[]{:S(2)}, u32[]{:S(2)}) collective-permute-start(bf16[256,2048]{1,0:T(8,128)(2,1)} %get-tuple-element.30.proj), channel_id=1, source_target_pairs={{0,1},{1,0},{2,3},{3,2},{4,5},{5,4},{6,7},{7,6},{8,9},{9,8},{10,11... | collective-permute-start | bytes 3145736 | tf_op jit(solution)/shard_map/ppermute | solution.py:437
  32.7 13.5 %all-to-all-start.1 = ((bf16[32,16,128]{2,1,0:T(8,128)(2,1)}), bf16[32,16,128]{2,1,0:T(8,128)(2,1)S(1)}, u32[]{:S(2)}, u32[]{:S(2)}) async-start(bf16[32,16,128]{2,1,0:T(8,128)(2,1)} %shard_map.202), calls=%async_computation.1 | async-start | bytes 262144 | tf_op jit(solution)/shard_map/all_to_all | solution.py:433
  46.6 5.7 %collective-permute-start = (bf16[128,256]{1,0:T(8,128)(2,1)S(1)}, bf16[128,256]{1,0:T(8,128)(2,1)S(1)}, u32[]{:S(2)}, u32[]{:S(2)}) collective-permute-start(bf16[128,256]{1,0:T(8,128)(2,1)S(1)} %get-tuple-element.29), channel_id=1, source_target_pairs={{0,1},{1,0},{2,3},{3,2},{4,5},{5,4},{6,7},{7,6},{8,9},{9,8},{10,11... | collective-permute-start | bytes 196616 | tf_op jit(solution)/shard_map/ppermute | solution.py:437
  52.2 27.6 %copy-start.3 = (f32[2048]{0:T(1024)S(1)}, f32[2048]{0:T(1024)}, u32[]{:S(2)}) copy-start(f32[2048]{0:T(1024)} %param.35) | copy-start | bytes 24580
  55.0 76.7 %copy-start.5 = (s32[256,2]{0,1:T(2,128)S(1)}, s32[256,2]{0,1:T(2,128)}, u32[]{:S(2)}) copy-start(s32[256,2]{0,1:T(2,128)} %param.37) | copy-start | bytes 6148
  55.0 76.7 %copy-start.6 = (f32[256,2]{0,1:T(2,128)S(1)}, f32[256,2]{0,1:T(2,128)}, u32[]{:S(2)}) copy-start(f32[256,2]{0,1:T(2,128)} %param.38) | copy-start | bytes 6148
  55.0 24.7 %all-to-all-start.2 = ((bf16[8,16,2048]{2,1,0:T(8,128)(2,1)}), bf16[8,16,2048]{2,1,0:T(8,128)(2,1)S(1)}, u32[]{:S(2)}, u32[]{:S(2)}) async-start(bf16[8,16,2048]{2,1,0:T(8,128)(2,1)} %bitcast.31), calls=%async_computation.2 | async-start | bytes 1048576 | tf_op jit(solution)/shard_map/all_to_all | solution.py:433
  62.0 67.2 %collective-permute-start.3 = (bf16[3072,256]{1,0:T(8,128)(2,1)S(1)}, bf16[3072,256]{1,0:T(8,128)(2,1)}, u32[]{:S(2)}, u32[]{:S(2)}) collective-permute-start(bf16[3072,256]{1,0:T(8,128)(2,1)S(1)} %get-tuple-element.32.own), channel_id=1, source_target_pairs={{0,2},{2,0},{1,3},{3,1},{4,6},{6,4},{5,7},{7,5},{8,10},{10,8},{9,1... | collective-permute-start | bytes 4718600 | tf_op jit(solution)/shard_map/ppermute | solution.py:437
  80.9 54.9 %copy-start.1 = (f32[16,2048]{1,0:T(8,128)}, f32[16,2048]{1,0:T(8,128)S(1)}, u32[]{:S(2)}) copy-start(f32[16,2048]{1,0:T(8,128)S(1)} %get-tuple-element.36.settled) | copy-start | bytes 393220
  124.9 8.2 %collective-permute-start.2 = (bf16[128,2048]{1,0:T(8,128)(2,1)S(1)}, bf16[128,2048]{1,0:T(8,128)(2,1)}, u32[]{:S(2)}, u32[]{:S(2)}) collective-permute-start(bf16[128,2048]{1,0:T(8,128)(2,1)S(1)} %bitcast.21), channel_id=1, source_target_pairs={{0,1},{1,0},{2,3},{3,2},{4,5},{5,4},{6,7},{7,6},{8,9},{9,8},{10,11... | collective-permute-start | bytes 1572872 | tf_op jit(solution)/shard_map/ppermute | solution.py:437
  127.3 12.4 %collective-permute-start.4 = (bf16[3072,256]{1,0:T(8,128)(2,1)S(1)}, bf16[3072,256]{1,0:T(8,128)(2,1)}, u32[]{:S(2)}, u32[]{:S(2)}) collective-permute-start(bf16[3072,256]{1,0:T(8,128)(2,1)S(1)} %get-tuple-element.32.own), channel_id=1, source_target_pairs={{0,1},{1,0},{2,3},{3,2},{4,5},{5,4},{6,7},{7,6},{8,9},{9,8},{10,11... | collective-permute-start | bytes 4718600 | tf_op jit(solution)/shard_map/ppermute | solution.py:437
  129.2 10.5 %collective-permute-start.5 = (bf16[3072,256]{1,0:T(8,128)(2,1)}, bf16[3072,256]{1,0:T(8,128)(2,1)}, u32[]{:S(2)}, u32[]{:S(2)}) collective-permute-start(bf16[3072,256]{1,0:T(8,128)(2,1)} %collective-permute-done.3.near), channel_id=1, source_target_pairs={{0,1},{1,0},{2,3},{3,2},{4,5},{5,4},{6,7},{7,6},{8,9},{9,8},{10,11... | collective-permute-start | bytes 4718600 | tf_op jit(solution)/shard_map/ppermute | solution.py:437
  135.8 26.2 %all-to-all-start.4 = ((bf16[32,24,512]{2,1,0:T(8,128)(2,1)}), bf16[32,24,512]{2,1,0:T(8,128)(2,1)S(1)}, u32[]{:S(2)}, u32[]{:S(2)}) async-start(bf16[32,24,512]{2,1,0:T(8,128)(2,1)} %bitcast.29), calls=%async_computation.4 | async-start | bytes 1572864 | tf_op jit(solution)/shard_map/all_to_all | solution.py:433
  194.1 6.3 %collective-permute-start.6 = (bf16[128,2048]{1,0:T(8,128)(2,1)S(1)}, bf16[128,2048]{1,0:T(8,128)(2,1)S(1)}, u32[]{:S(2)}, u32[]{:S(2)}) collective-permute-start(bf16[128,2048]{1,0:T(8,128)(2,1)S(1)} %get-tuple-element.35), channel_id=1, source_target_pairs={{0,1},{1,0},{2,3},{3,2},{4,5},{5,4},{6,7},{7,6},{8,9},{9,8},{10,11... | collective-permute-start | bytes 1572872 | tf_op jit(solution)/shard_map/ppermute | solution.py:437
  200.4 22.2 %copy-start.2 = (f32[16,2048]{1,0:T(8,128)S(1)}, f32[16,2048]{1,0:T(8,128)}, u32[]{:S(2)}) copy-start(f32[16,2048]{1,0:T(8,128)} %copy-done.1) | copy-start | bytes 393220
  200.4 22.2 %copy-start.4 = (f32[2048]{0:T(1024)S(1)}, f32[2048]{0:T(1024)}, u32[]{:S(2)}) copy-start(f32[2048]{0:T(1024)} %param.36) | copy-start | bytes 24580

commit v2 on v1

--- a/solution.py
+++ b/solution.py
@@ -13,6 +13,8 @@
 SHARERS = 4
 SLOTS = 6
 STEP = 16
+SPLIT = 1
+LINES = SHARERS * SLOTS
 SP = ("z", "x")
 Y = ("p", "b")
 TP = ("p", "b", "c")
@@ -20,7 +22,7 @@
 SWAP = [(0, 1), (1, 0)]
 F32 = jnp.float32
 BF16 = jnp.bfloat16
-VMEM_LIMIT = 16 * 1024 * 1024
+VMEM_LIMIT = 32 * 1024 * 1024
 normalizer_sharpness = 16.0
 
 
@@ -85,24 +87,9 @@
 
 
 def states_kernel(
-    d1h, d2h, k1h, v1h, k2h, v2h, gate, up, down, one, two,
-    pieces, pack, proj,
-    d1, d2, k1, v1, k2, v2, spread, marks, moves,
+    d1h, d2h, k1h, v1h, k2h, v2h, pieces, d1, d2, k1, v1, k2, v2, spread, marks
 ):
     copies = fetched((d1h, d2h, k1h, v1h, k2h, v2h), (d1, d2, k1, v1, k2, v2), marks)
-    features, hidden = gate.shape[1:]
-    blocks = down.shape[2] // (2 * hidden)
-    sources = [gate.at[0], up.at[0], one, two]
-    places = [
-        pack.at[:features, :hidden],
-        pack.at[:features, hidden:],
-        proj.at[:hidden, :],
-        proj.at[hidden:, :],
-    ]
-    for n in range(blocks):
-        sources.append(down.at[0, :, 2 * hidden * n : 2 * hidden * (n + 1)])
-        places.append(pack.at[features + hidden * n : features + hidden * (n + 1), :])
-    moved = fetched(sources, places, moves)
     size, length = k1.shape
     peers = spread.shape[0] // 24
     row, col = grid_of(length)
@@ -140,7 +127,24 @@
     put(fast_dot(key * wide_f, value, across), 0, size // peers)
     put(fast_dot(key * wide_b, value, across), 1, size // peers)
     pieces[...] = spread[...].astype(BF16)
-    for copy in moved:
+
+
+def pack_kernel(where, gate, up, down, one, two, stream, pack, proj, own, moves):
+    features, hidden = gate.shape[1:]
+    sources = [gate.at[0], up.at[0], one, two]
+    places = [
+        pack.at[:features, :hidden],
+        pack.at[:features, hidden:],
+        proj.at[:hidden, :],
+        proj.at[hidden:, :],
+    ]
+    for n in range(down.shape[2] // (2 * hidden)):
+        sources.append(down.at[0, :, 2 * hidden * n : 2 * hidden * (n + 1)])
+        places.append(pack.at[features + hidden * n : features + hidden * (n + 1), :])
+    rows = own.shape[0]
+    sources.append(stream.at[pl.ds(pl.multiple_of(where[0] * rows, rows), rows), :])
+    places.append(own)
+    for copy in fetched(sources, places, moves):
         copy.wait()
 
 
@@ -324,16 +328,17 @@
         packed[:, n * 128 : (n + 1) * 128] = spread[n].astype(BF16)
 
 
-def strided(part, slot, peers):
-    return pl.ds(part * SLOTS + slot, peers, stride=SHARERS * SLOTS)
-
-
-def taken(spread, part):
-    peers = spread.shape[1] // (SHARERS * SLOTS)
+def strided(first, peers):
+    return pl.ds(first, peers, stride=LINES)
+
+
+def taken(spread, part, each):
+    peers = spread.shape[1] // LINES
     return jnp.concatenate(
         [
             jnp.concatenate(
-                [spread[n, strided(part, slot, peers), :] for slot in range(SLOTS)], axis=0
+                [spread[n, strided(part * each + slot, peers), :] for slot in range(each)],
+                axis=0,
             ).astype(BF16)
             for n in range(spread.shape[0])
         ],
@@ -341,55 +346,71 @@
     )
 
 
-def placed(spread, part, value, lane):
-    peers = spread.shape[1] // (SHARERS * SLOTS)
+def placed(spread, part, each, value):
+    peers = spread.shape[1] // LINES
     for n in range(value.shape[1] // 128):
-        for slot in range(SLOTS):
-            spread[lane + n, strided(part, slot, peers), :] = value[
+        for slot in range(each):
+            spread[n, strided(part * each + slot, peers), :] = value[
                 slot * peers : (slot + 1) * peers, n * 128 : (n + 1) * 128
             ]
 
 
 def dispatch_kernel(chosen, own, other, out, spread):
     wide = out.shape[1]
-    for part in range(SHARERS):
+    each = SLOTS // SPLIT
+    for part in range(LINES // each):
         lanes = slice(part * wide, (part + 1) * wide)
         both = jnp.concatenate([own[:, lanes], other[:, lanes]], axis=0)
-        placed(spread, part, fast_dot(chosen[...], both), 0)
+        placed(spread, part, each, fast_dot(chosen[...], both))
     tighten(spread, out)
 
 
-def expert_kernel(rows, own, near, side, far, out, spread):
+def expert_kernel(
+    rows, own, near, side, far, out, spread, own_here, near_here, side_here, far_here, marks
+):
+    packs = (own_here, near_here, side_here, far_here)
+    copies = fetched((own, near, side, far), packs, marks)
     wide = rows.shape[1]
     hidden = own.shape[1] // 2
-    packs = (own, near, side, far)
+    each = SLOTS // SPLIT
+    parts = LINES // each
     loosen(rows, spread)
-    x = jnp.concatenate([taken(spread, part) for part in range(SHARERS)], axis=1)
-    features = SHARERS * wide
+    x = jnp.concatenate([taken(spread, part, each) for part in range(parts)], axis=1)
+    features = parts * wide
     acts = []
-    for pack in packs:
+    for copy, pack in zip(copies, packs):
+        copy.wait()
         both = fast_dot(x, pack[:features, :])
         gate, upward = both[:, :hidden], both[:, hidden:]
         acts.append((gate * jax.nn.sigmoid(gate) * upward).astype(BF16))
     acts = [jnp.concatenate(acts[:2], axis=1), jnp.concatenate(acts[2:], axis=1)]
     step = 2 * hidden
+    found = []
     for n in range(features // step):
         here = slice(features + n * hidden, features + (n + 1) * hidden)
         value = 0.0
         for act, pair in zip(acts, (packs[:2], packs[2:])):
             value = value + fast_dot(act, jnp.concatenate([pack[here, :] for pack in pair], axis=0))
-        placed(spread, n * step // wide, value, n * step % wide // 128)
+        found.append(value)
+        if (n + 1) * step % wide == 0:
+            placed(spread, n * step // wide, each, jnp.concatenate(found, axis=1))
+            found = []
     tighten(spread, out)
 
 
-def combine_kernel(weighted, returned, own, sent, spread):
+def combine_kernel(weighted, *refs):
+    returned, own, sent, spread = refs[:SPLIT], refs[SPLIT], refs[SPLIT + 1], refs[SPLIT + 2 :]
     half = own.shape[0]
-    wide = returned.shape[1]
-    loosen(returned, spread)
-    for part in range(SHARERS):
-        value = fast_dot(weighted[...], taken(spread, part))
-        own[:, part * wide : (part + 1) * wide] = value[:half]
-        sent[:, part * wide : (part + 1) * wide] = value[half:].astype(BF16)
+    wide = returned[0].shape[1]
+    each = SLOTS // SPLIT
+    for packed, held in zip(returned, spread):
+        loosen(packed, held)
+    for part in range(LINES // each):
+        lanes = slice(part * wide, (part + 1) * wide)
+        rows = jnp.concatenate([taken(held, part, each) for held in spread], axis=0)
+        value = fast_dot(weighted[...], rows)
+        own[:, lanes] = value[:half]
+        sent[:, lanes] = value[half:].astype(BF16)
 
 
 def settle_kernel(parts, stream, gain, settled, copies):
@@ -414,12 +435,15 @@
     out[...] = (own[...] + got[...].astype(F32)).astype(BF16)
 
 
-def project_kernel(own, got, proj, other, out):
+def project_kernel(own, got, proj, other, out, proj_here, marks):
+    copies = fetched((proj,), (proj_here,), marks)
+    theirs = fast_dot(got[...], other[...])
+    copies[0].wait()
     width = out.shape[1]
     step = width // 4
     for n in range(4):
         lanes = slice(n * step, (n + 1) * step)
-        value = fast_dot(own[...], proj[:, lanes]) + fast_dot(got[...], other[:, lanes])
+        value = theirs[:, lanes] + fast_dot(own[...], proj_here[:, lanes])
         out[:, lanes] = value.astype(BF16)
 
 
@@ -524,8 +548,8 @@
     group = lax.axis_index(("b", "c"))
     hidden = expert_gate.shape[2]
     slots = peers * SLOTS
-    total = SHARERS * slots
-    wide = width // SHARERS
+    each = slots // SPLIT
+    wide = width * SLOTS // SPLIT // LINES
     keys = DK_A + DK_B
     shape = jax.ShapeDtypeStruct
 
@@ -534,28 +558,33 @@
         return held, pltpu.SemaphoreType.DMA((len(items),))
 
     early = (decay_one, decay_two, key_one, value_one, key_two, value_two)
-    moves = (expert_gate, expert_up, expert_down, proj_one, proj_two)
+    moves = (expert_gate, expert_up, expert_down, proj_one, proj_two, stream)
     held, marks = scratch(early)
-    lines = 4 * keys
+    pieces_rows = 4 * keys
     blocks = width // (2 * hidden)
-    pieces, pack, proj = call(
+    pieces = call(
         states_kernel,
+        pltpu.HBM((pieces_rows, 128), BF16),
+        *early,
+        far=range(len(early)),
+        scratch=held + [pltpu.VMEM((pieces_rows, 128), F32), marks],
+    )
+    arrived = exchange(pieces.reshape(peers, pieces_rows // peers, 128), SP)
+    pack, proj, stream_own = call(
+        pack_kernel,
         [
-            pltpu.HBM((lines, 128), BF16),
-            shape((width + blocks * hidden, 2 * hidden), BF16),
-            shape((2 * hidden, width), BF16),
+            pltpu.HBM((width + blocks * hidden, 2 * hidden), BF16),
+            pltpu.HBM((2 * hidden, width), BF16),
+            shape((own_rows, width), BF16),
         ],
-        *early,
+        tp_rank.reshape(1).astype(jnp.int32),
         *moves,
-        far=range(len(early) + len(moves)),
-        scratch=held
-        + [pltpu.VMEM((lines, 128), F32), marks, pltpu.SemaphoreType.DMA((4 + blocks,))],
-    )
-    pieces = pieces.reshape(peers, lines // peers, 128)
+        far=range(1, 1 + len(moves)),
+        scratch=[pltpu.SemaphoreType.DMA((5 + blocks,))],
+    )
     near = swapped(pack, "b")
     side = swapped(pack, "c")
     proj_other = swapped(proj, "c")
-    arrived = exchange(pieces, SP)
     late = (
         query_one,
         key_one,
@@ -584,7 +613,7 @@
     )
     chosen, weighted = call(
         routing_kernel,
-        [shape((slots, rows), BF16), shape((rows, slots), BF16)],
+        [pltpu.HBM((slots, rows), BF16), pltpu.HBM((rows, slots), BF16)],
         jnp.stack([core, group * SLOTS]).astype(jnp.int32),
         routes.T,
         affinity.T,
@@ -607,46 +636,59 @@
     far = swapped(tied(near, heads_own), "c")
     heads_got = swapped(heads_sent, "c")
     part = call(
-        project_kernel, pltpu.HBM((half, width), BF16), heads_own, heads_got, proj, proj_other
+        project_kernel,
+        pltpu.HBM((half, width), BF16),
+        heads_own,
+        heads_got,
+        proj,
+        proj_other,
+        far=(2,),
+        scratch=[pltpu.VMEM((2 * hidden, width), BF16), pltpu.SemaphoreType.DMA((1,))],
     )
     attn = exchange(part.reshape(chips, own_rows, width), Y)
-    stream_own = lax.dynamic_slice_in_dim(stream, tp_rank * own_rows, own_rows, 0)
     settled, mine = call(
         settle_kernel,
-        [shape((own_rows, width), F32), pltpu.HBM((chips, own_rows, width), BF16)],
+        [pltpu.HBM((own_rows, width), F32), pltpu.HBM((chips, own_rows, width), BF16)],
         attn,
         stream_own,
         gain_mix.reshape(1, width),
     )
     moe_own = exchange(mine, Y).reshape(half, width)
     moe_other = swapped(moe_own, "c")
-    spread = [pltpu.VMEM((wide // 128, total, 128), F32)]
-    outgoing = call(
-        dispatch_kernel,
-        pltpu.HBM((total, wide), BF16),
-        chosen,
-        moe_own,
-        moe_other,
-        scratch=spread,
-    )
-    complete = exchange(outgoing.reshape(peers, total // peers, wide), SP)
-    partial = call(
-        expert_kernel,
-        pltpu.HBM((total, wide), BF16),
-        complete.reshape(total, wide),
-        pack,
-        near,
-        side,
-        far,
-        scratch=spread,
-    )
-    returned = exchange(partial.reshape(peers, total // peers, wide), SP)
+    lines = peers * LINES
+    spread = [pltpu.VMEM((wide // 128, lines, 128), F32)]
+    returned = []
+    for turn in range(SPLIT):
+        outgoing = call(
+            dispatch_kernel,
+            pltpu.HBM((lines, wide), BF16),
+            chosen[turn * each : (turn + 1) * each],
+            moe_own,
+            moe_other,
+            scratch=spread,
+        )
+        complete = exchange(outgoing.reshape(peers, LINES, wide), SP)
+        partial = call(
+            expert_kernel,
+            pltpu.HBM((lines, wide), BF16),
+            complete.reshape(lines, wide),
+            pack,
+            near,
+            side,
+            far,
+            far=range(1, 5),
+            scratch=spread
+            + [pltpu.VMEM(pack.shape, BF16)] * 4
+            + [pltpu.SemaphoreType.DMA((4,))],
+        )
+        arrived = exchange(partial.reshape(peers, LINES, wide), SP)
+        returned.append(arrived.reshape(lines, wide))
     term_own, term_sent = call(
         combine_kernel,
         [shape((half, width), F32), shape((half, width), BF16)],
         weighted,
-        returned.reshape(total, wide),
-        scratch=spread,
+        *returned,
+        scratch=spread * SPLIT,
     )
     term = call(join_kernel, pltpu.HBM((half, width), BF16), term_own, swapped(term_sent, "c"))
     mixture = exchange(term.reshape(chips, own_rows, width), Y)

time: 224 us -> 227 us (1.013)
    pallas_call x12 -> x13, Pallas kernels: 26.2 us -> 27.7 us  [call(): pl.pallas_call(kernel, out_shape=shapes, in_specs=[pl.BlockSpec(memory_sp...]
  transfers between devices with their start and end apart: 10 -> 10, of which waited for: 5 -> 5; matrix products, arithmetic and copies ran while one was open for 0% -> 0% of each run, Pallas kernels for 5% -> 6%
where the time goes in v2:
time: 227 us; the launch traced here: 226 us
  blocking collectives  110 us (48%)
  waiting for transfers between devices  43.7 us (19%)
  starting transfers between devices  43.3 us (19%)
  Pallas kernels  27.7 us (12%)
    all_to_all x4, blocking collectives, exchange(): return lax.all_to_all(pieces, axis, split_axis=0, concat_axis=0, tiled=True)  110 us
    all_to_all x3, waiting for transfers between devices, exchange(): return lax.all_to_all(pieces, axis, split_axis=0, concat_axis=0, tiled=True)  41.3 us
    ppermute x7, starting transfers between devices, swapped(): return lax.ppermute(value, axis, SWAP)  28.4 us
    pallas_call x13, Pallas kernels, call(): pl.pallas_call(kernel, out_shape=shapes, in_specs=[pl.BlockSpec(memory_sp...  27.7 us
    all_to_all x3, starting transfers between devices, exchange(): return lax.all_to_all(pieces, axis, split_axis=0, concat_axis=0, tiled=True)  14.9 us
  transfers between devices with their start and end apart: 10, of which 5 were waited for; matrix products, arithmetic and copies ran while one was open for 0% of the time, Pallas kernels for 6%

profile of v2, /device:TPU:1, one launch (start us, length us, event | category | flops | bytes accessed | tf_op | source)
XLA Modules:
  0.0 226.0 jit_solution(5823721440357756532)
XLA Ops:
  0.0 3.3 %shard_map.204 = (bf16[3072,256]{1,0:T(8,128)(2,1)}, bf16[256,2048]{1,0:T(8,128)(2,1)}, bf16[16,2048]{1,0:T(8,128)(2,1)S(1)}) custom-call(s32[1]{0:T(128)} %bitcast.10.where, bf16[1,2048,128]{2,1,0:T(8,128)(2,1)} %gate.1, bf16[1,2048,128]{2,1,0:T(8,128)(2,1)} %up.1, bf16[1,128,2048]{2,1,0:T(8,128)(2,1)} %down.1, bf16[128,2048]{1,0:T(8,128)(2,1)} %one.1, ...), custom_call_target="tpu_custom_call" | custom-call | tf_op jit(solution)/shard_map/pallas_call | solution.py:34
  3.3 8.7 %collective-permute-start.1 = (bf16[256,2048]{1,0:T(8,128)(2,1)}, bf16[256,2048]{1,0:T(8,128)(2,1)S(1)}, u32[]{:S(2)}, u32[]{:S(2)}) collective-permute-start(bf16[256,2048]{1,0:T(8,128)(2,1)} %get-tuple-element.29.proj), channel_id=1, source_target_pairs={{0,1},{1,0},{2,3},{3,2},{4,5},{5,4},{6,7},{7,6},{8,9},{9,8},{10,11... | collective-permute-start | bytes 3145736 | tf_op jit(solution)/shard_map/ppermute | solution.py:461
  12.0 3.6 %shard_map.201 = bf16[768,128]{1,0:T(8,128)(2,1)} custom-call(f32[2,64,256]{2,1,0:T(8,128)} %bitcast.35, f32[2,256,128]{2,1,0:T(8,128)} %d2h.3, bf16[64,256]{1,0:T(8,128)(2,1)} %bitcast.37, bf16[256,128]{1,0:T(8,128)(2,1)} %v1h.3, bf16[256,128]{1,0:T(8,128)(2,1)} %k2h.3, bf16[256,128]{1,0:T(8,128)(2,1)} %v2h.3), custom_call_target="tpu_custom_call" | custom-call | tf_op jit(solution)/shard_map/pallas_call | solution.py:34
  15.6 18.3 %all_to_all.35.pieces = bf16[32,24,128]{2,1,0:T(8,128)(2,1)S(1)} all-to-all(bf16[32,24,128]{2,1,0:T(8,128)(2,1)} %bitcast.34), channel_id=1, replica_groups=mesh['z'=8,'x'=4,'p'=4,'b'=2,'c'=2] {'z','x'}, dimensions={0} | all-to-all | bytes 393216 | tf_op jit(solution)/shard_map/all_to_all | solution.py:457
  33.9 0.8 shard_map.202
  34.7 4.1 %all-to-all-start.1 = ((bf16[32,16,128]{2,1,0:T(8,128)(2,1)}), bf16[32,16,128]{2,1,0:T(8,128)(2,1)S(1)}, u32[]{:S(2)}, u32[]{:S(2)}) async-start(bf16[32,16,128]{2,1,0:T(8,128)(2,1)} %shard_map.202), calls=%async_computation.1 | async-start | bytes 262144 | tf_op jit(solution)/shard_map/all_to_all | solution.py:457
  38.8 4.7 %shard_map.200 = (f32[256,256]{1,0:T(8,128)S(1)}, bf16[256,128]{1,0:T(8,128)(2,1)S(1)}, bf16[256,256]{1,0:T(8,128)(2,1)S(1)}, f32[256,256]{1,0:T(8,128)S(1)}) custom-call(bf16[64,256]{1,0:T(8,128)(2,1)} %bitcast.39, bf16[64,256]{1,0:T(8,128)(2,1)} %bitcast.38, bf16[256,128]{1,0:T(8,128)(2,1)} %v1h.3, f32[2,64,256]{2,1,0:T(8,128)} %bitcast.36, ...), custom_call_target="tpu_custom_call" | custom-call | tf_op jit(solution)/shard_map/pallas_call | solution.py:34
  43.6 4.6 %all-to-all-done.1 = bf16[32,16,128]{2,1,0:T(8,128)(2,1)S(1)} async-done(((bf16[32,16,128]{2,1,0:T(8,128)(2,1)}), bf16[32,16,128]{2,1,0:T(8,128)(2,1)S(1)}, u32[]{:S(2)}, u32[]{:S(2)}) %all-to-all-start.1) | async-done | bytes 131104 | tf_op jit(solution)/shard_map/all_to_all | solution.py:457
  48.5 4.8 %collective-permute-start = (bf16[128,256]{1,0:T(8,128)(2,1)S(1)}, bf16[128,256]{1,0:T(8,128)(2,1)S(1)}, u32[]{:S(2)}, u32[]{:S(2)}) collective-permute-start(bf16[128,256]{1,0:T(8,128)(2,1)S(1)} %get-tuple-element.28), channel_id=1, source_target_pairs={{0,1},{1,0},{2,3},{3,2},{4,5},{5,4},{6,7},{7,6},{8,9},{9,8},{10,11... | collective-permute-start | bytes 196616 | tf_op jit(solution)/shard_map/ppermute | solution.py:461
  53.3 0.9 collective-permute-done.got
  54.2 2.5 %shard_map.205 = bf16[128,2048]{1,0:T(8,128)(2,1)} custom-call(bf16[128,256]{1,0:T(8,128)(2,1)S(1)} %get-tuple-element.27.own, bf16[128,256]{1,0:T(8,128)(2,1)S(1)} %collective-permute-done.got, bf16[256,2048]{1,0:T(8,128)(2,1)} %get-tuple-element.29.proj, bf16[256,2048]{1,0:T(8,128)(2,1)S(1)} %collective-permute-done.1.other), custom_call_target="tpu_custom_call" | custom-call | tf_op jit(solution)/shard_map/pallas_call | solution.py:34
  56.7 6.8 %all-to-all-start.2 = ((bf16[8,16,2048]{2,1,0:T(8,128)(2,1)}), bf16[8,16,2048]{2,1,0:T(8,128)(2,1)S(1)}, u32[]{:S(2)}, u32[]{:S(2)}) async-start(bf16[8,16,2048]{2,1,0:T(8,128)(2,1)} %bitcast.32), calls=%async_computation.2 | async-start | bytes 1048576 | tf_op jit(solution)/shard_map/all_to_all | solution.py:457
  63.6 3.4 %collective-permute-start.3 = (bf16[3072,256]{1,0:T(8,128)(2,1)S(1)}, bf16[3072,256]{1,0:T(8,128)(2,1)}, u32[]{:S(2)}, u32[]{:S(2)}) collective-permute-start(bf16[3072,256]{1,0:T(8,128)(2,1)S(1)} %copy-done.8), channel_id=1, source_target_pairs={{0,2},{2,0},{1,3},{3,1},{4,6},{6,4},{5,7},{7,5},{8,10},{10,8},{9,1... | collective-permute-start | bytes 4718600 | tf_op jit(solution)/shard_map/ppermute | solution.py:461
  66.9 14.4 %all-to-all-done.2.parts = bf16[8,16,2048]{2,1,0:T(8,128)(2,1)S(1)} async-done(((bf16[8,16,2048]{2,1,0:T(8,128)(2,1)}), bf16[8,16,2048]{2,1,0:T(8,128)(2,1)S(1)}, u32[]{:S(2)}, u32[]{:S(2)}) %all-to-all-start.2) | async-done | bytes 524320 | tf_op jit(solution)/shard_map/all_to_all | solution.py:457
  81.4 1.1 shard_map.206
  82.5 44.0 %all_to_all.36 = bf16[8,16,2048]{2,1,0:T(8,128)(2,1)S(1)} all-to-all(bf16[8,16,2048]{2,1,0:T(8,128)(2,1)} %get-tuple-element.31), channel_id=1, replica_groups=mesh['z'=8,'x'=4,'p'=4,'b'=2,'c'=2] {'p','b'}, dimensions={0} | all-to-all | bytes 1048576 | tf_op jit(solution)/shard_map/all_to_all | solution.py:457
  126.5 2.4 %collective-permute-start.2 = (bf16[128,2048]{1,0:T(8,128)(2,1)S(1)}, bf16[128,2048]{1,0:T(8,128)(2,1)S(1)}, u32[]{:S(2)}, u32[]{:S(2)}) collective-permute-start(bf16[128,2048]{1,0:T(8,128)(2,1)S(1)} %bitcast.22), channel_id=1, source_target_pairs={{0,1},{1,0},{2,3},{3,2},{4,5},{5,4},{6,7},{7,6},{8,9},{9,8},{10,11... | collective-permute-start | bytes 1572872 | tf_op jit(solution)/shard_map/ppermute | solution.py:461
  128.9 1.9 collective-permute-start.4
  130.8 2.4 %collective-permute-start.5 = (bf16[3072,256]{1,0:T(8,128)(2,1)}, bf16[3072,256]{1,0:T(8,128)(2,1)}, u32[]{:S(2)}, u32[]{:S(2)}) collective-permute-start(bf16[3072,256]{1,0:T(8,128)(2,1)} %collective-permute-done.3.near), channel_id=1, source_target_pairs={{0,1},{1,0},{2,3},{3,2},{4,5},{5,4},{6,7},{7,6},{8,9},{9,8},{10,11... | collective-permute-start | bytes 4718600 | tf_op jit(solution)/shard_map/ppermute | solution.py:461
  133.3 2.0 shard_map.199
  135.4 0.9 copy-done.2
  136.3 1.6 shard_map.207
  137.8 3.9 %all-to-all-start.4 = ((bf16[32,24,512]{2,1,0:T(8,128)(2,1)}), bf16[32,24,512]{2,1,0:T(8,128)(2,1)S(1)}, u32[]{:S(2)}, u32[]{:S(2)}) async-start(bf16[32,24,512]{2,1,0:T(8,128)(2,1)} %bitcast.30), calls=%async_computation.4 | async-start | bytes 1572864 | tf_op jit(solution)/shard_map/all_to_all | solution.py:457
  141.8 22.3 %all-to-all-done.4 = bf16[32,24,512]{2,1,0:T(8,128)(2,1)S(1)} async-done(((bf16[32,24,512]{2,1,0:T(8,128)(2,1)}), bf16[32,24,512]{2,1,0:T(8,128)(2,1)S(1)}, u32[]{:S(2)}, u32[]{:S(2)}) %all-to-all-start.4) | async-done | bytes 786464 | tf_op jit(solution)/shard_map/all_to_all | solution.py:457
  164.0 5.3 %shard_map.208 = bf16[768,512]{1,0:T(8,128)(2,1)} custom-call(bf16[768,512]{1,0:T(8,128)(2,1)S(1)} %bitcast.21, bf16[3072,256]{1,0:T(8,128)(2,1)} %get-tuple-element.32.own, bf16[3072,256]{1,0:T(8,128)(2,1)} %collective-permute-done.3.near, bf16[3072,256]{1,0:T(8,128)(2,1)} %collective-permute-done.4.side, bf16[3072,256]{1,0:T(8,128)(2,1)} %collective-permute-done.5.far), custom_call_target="tpu_custom_call" | custom-call | tf_op jit(solution)/shard_map/pallas_call | solution.py:34
  169.3 26.6 %all_to_all.37 = bf16[32,24,512]{2,1,0:T(8,128)(2,1)S(1)} all-to-all(bf16[32,24,512]{2,1,0:T(8,128)(2,1)} %bitcast.31), channel_id=1, replica_groups=mesh['z'=8,'x'=4,'p'=4,'b'=2,'c'=2] {'z','x'}, dimensions={0} | all-to-all | bytes 1572864 | tf_op jit(solution)/shard_map/all_to_all | solution.py:457
  195.9 0.6 shard_map.209
  196.5 4.8 %collective-permute-start.6 = (bf16[128,2048]{1,0:T(8,128)(2,1)S(1)}, bf16[128,2048]{1,0:T(8,128)(2,1)S(1)}, u32[]{:S(2)}, u32[]{:S(2)}) collective-permute-start(bf16[128,2048]{1,0:T(8,128)(2,1)S(1)} %get-tuple-element.35), channel_id=1, source_target_pairs={{0,1},{1,0},{2,3},{3,2},{4,5},{5,4},{6,7},{7,6},{8,9},{9,8},{10,11... | collective-permute-start | bytes 1572872 | tf_op jit(solution)/shard_map/ppermute | solution.py:461
  201.3 1.5 collective-permute-done.6.got
  202.8 0.9 shard_map.210
  203.7 21.3 %all_to_all.38.parts = bf16[8,16,2048]{2,1,0:T(8,128)(2,1)S(1)} all-to-all(bf16[8,16,2048]{2,1,0:T(8,128)(2,1)} %bitcast.33), channel_id=1, replica_groups=mesh['z'=8,'x'=4,'p'=4,'b'=2,'c'=2] {'p','b'}, dimensions={0} | all-to-all | bytes 1048576 | tf_op jit(solution)/shard_map/all_to_all | solution.py:457
  225.1 0.9 shard_map.211
  (24 shorter events, 0.5 us)
Async XLA Ops:
  3.3 35.6 %copy-start.7 = (f32[128]{0:T(128)S(1)}, f32[128]{0:T(128)}, u32[]{:S(2)}) copy-start(f32[128]{0:T(128)} %param.31) | copy-start | bytes 1540
  3.3 50.9 %collective-permute-start.1 = (bf16[256,2048]{1,0:T(8,128)(2,1)}, bf16[256,2048]{1,0:T(8,128)(2,1)S(1)}, u32[]{:S(2)}, u32[]{:S(2)}) collective-permute-start(bf16[256,2048]{1,0:T(8,128)(2,1)} %get-tuple-element.29.proj), channel_id=1, source_target_pairs={{0,1},{1,0},{2,3},{3,2},{4,5},{5,4},{6,7},{7,6},{8,9},{9,8},{10,11... | collective-permute-start | bytes 3145736 | tf_op jit(solution)/shard_map/ppermute | solution.py:461
  34.7 13.5 %all-to-all-start.1 = ((bf16[32,16,128]{2,1,0:T(8,128)(2,1)}), bf16[32,16,128]{2,1,0:T(8,128)(2,1)S(1)}, u32[]{:S(2)}, u32[]{:S(2)}) async-start(bf16[32,16,128]{2,1,0:T(8,128)(2,1)} %shard_map.202), calls=%async_computation.1 | async-start | bytes 262144 | tf_op jit(solution)/shard_map/all_to_all | solution.py:457
  48.5 5.7 %collective-permute-start = (bf16[128,256]{1,0:T(8,128)(2,1)S(1)}, bf16[128,256]{1,0:T(8,128)(2,1)S(1)}, u32[]{:S(2)}, u32[]{:S(2)}) collective-permute-start(bf16[128,256]{1,0:T(8,128)(2,1)S(1)} %get-tuple-element.28), channel_id=1, source_target_pairs={{0,1},{1,0},{2,3},{3,2},{4,5},{5,4},{6,7},{7,6},{8,9},{9,8},{10,11... | collective-permute-start | bytes 196616 | tf_op jit(solution)/shard_map/ppermute | solution.py:461
  54.2 9.4 %copy-start.8 = (bf16[3072,256]{1,0:T(8,128)(2,1)S(1)}, bf16[3072,256]{1,0:T(8,128)(2,1)}, u32[]{:S(2)}) copy-start(bf16[3072,256]{1,0:T(8,128)(2,1)} %get-tuple-element.32.own) | copy-start | bytes 4718596
  54.2 27.1 %copy-start.3 = (f32[2048]{0:T(1024)S(1)}, f32[2048]{0:T(1024)}, u32[]{:S(2)}) copy-start(f32[2048]{0:T(1024)} %param.35) | copy-start | bytes 24580
  56.7 76.6 %copy-start.5 = (s32[256,2]{0,1:T(2,128)S(1)}, s32[256,2]{0,1:T(2,128)}, u32[]{:S(2)}) copy-start(s32[256,2]{0,1:T(2,128)} %param.37) | copy-start | bytes 6148
  56.7 76.6 %copy-start.6 = (f32[256,2]{0,1:T(2,128)S(1)}, f32[256,2]{0,1:T(2,128)}, u32[]{:S(2)}) copy-start(f32[256,2]{0,1:T(2,128)} %param.38) | copy-start | bytes 6148
  56.7 24.6 %all-to-all-start.2 = ((bf16[8,16,2048]{2,1,0:T(8,128)(2,1)}), bf16[8,16,2048]{2,1,0:T(8,128)(2,1)S(1)}, u32[]{:S(2)}, u32[]{:S(2)}) async-start(bf16[8,16,2048]{2,1,0:T(8,128)(2,1)} %bitcast.32), calls=%async_computation.2 | async-start | bytes 1048576 | tf_op jit(solution)/shard_map/all_to_all | solution.py:457
  63.6 67.2 %collective-permute-start.3 = (bf16[3072,256]{1,0:T(8,128)(2,1)S(1)}, bf16[3072,256]{1,0:T(8,128)(2,1)}, u32[]{:S(2)}, u32[]{:S(2)}) collective-permute-start(bf16[3072,256]{1,0:T(8,128)(2,1)S(1)} %copy-done.8), channel_id=1, source_target_pairs={{0,2},{2,0},{1,3},{3,1},{4,6},{6,4},{5,7},{7,5},{8,10},{10,8},{9,1... | collective-permute-start | bytes 4718600 | tf_op jit(solution)/shard_map/ppermute | solution.py:461
  126.5 8.9 %collective-permute-start.2 = (bf16[128,2048]{1,0:T(8,128)(2,1)S(1)}, bf16[128,2048]{1,0:T(8,128)(2,1)S(1)}, u32[]{:S(2)}, u32[]{:S(2)}) collective-permute-start(bf16[128,2048]{1,0:T(8,128)(2,1)S(1)} %bitcast.22), channel_id=1, source_target_pairs={{0,1},{1,0},{2,3},{3,2},{4,5},{5,4},{6,7},{7,6},{8,9},{9,8},{10,11... | collective-permute-start | bytes 1572872 | tf_op jit(solution)/shard_map/ppermute | solution.py:461
  128.9 12.9 %collective-permute-start.4 = (bf16[3072,256]{1,0:T(8,128)(2,1)S(1)}, bf16[3072,256]{1,0:T(8,128)(2,1)}, u32[]{:S(2)}, u32[]{:S(2)}) collective-permute-start(bf16[3072,256]{1,0:T(8,128)(2,1)S(1)} %copy-done.8), channel_id=1, source_target_pairs={{0,1},{1,0},{2,3},{3,2},{4,5},{5,4},{6,7},{7,6},{8,9},{9,8},{10,11... | collective-permute-start | bytes 4718600 | tf_op jit(solution)/shard_map/ppermute | solution.py:461
  130.8 10.9 %collective-permute-start.5 = (bf16[3072,256]{1,0:T(8,128)(2,1)}, bf16[3072,256]{1,0:T(8,128)(2,1)}, u32[]{:S(2)}, u32[]{:S(2)}) collective-permute-start(bf16[3072,256]{1,0:T(8,128)(2,1)} %collective-permute-done.3.near), channel_id=1, source_target_pairs={{0,1},{1,0},{2,3},{3,2},{4,5},{5,4},{6,7},{7,6},{8,9},{9,8},{10,11... | collective-permute-start | bytes 4718600 | tf_op jit(solution)/shard_map/ppermute | solution.py:461
  135.4 0.9 copy-start.2
  137.8 26.2 %all-to-all-start.4 = ((bf16[32,24,512]{2,1,0:T(8,128)(2,1)}), bf16[32,24,512]{2,1,0:T(8,128)(2,1)S(1)}, u32[]{:S(2)}, u32[]{:S(2)}) async-start(bf16[32,24,512]{2,1,0:T(8,128)(2,1)} %bitcast.30), calls=%async_computation.4 | async-start | bytes 1572864 | tf_op jit(solution)/shard_map/all_to_all | solution.py:457
  169.3 26.6 %copy-start = (bf16[256,192]{1,0:T(8,128)(2,1)S(1)}, bf16[256,192]{1,0:T(8,128)(2,1)}, u32[]{:S(2)}) copy-start(bf16[256,192]{1,0:T(8,128)(2,1)} %get-tuple-element.21.weighted) | copy-start | bytes 294916
  196.5 6.3 %collective-permute-start.6 = (bf16[128,2048]{1,0:T(8,128)(2,1)S(1)}, bf16[128,2048]{1,0:T(8,128)(2,1)S(1)}, u32[]{:S(2)}, u32[]{:S(2)}) collective-permute-start(bf16[128,2048]{1,0:T(8,128)(2,1)S(1)} %get-tuple-element.35), channel_id=1, source_target_pairs={{0,1},{1,0},{2,3},{3,2},{4,5},{5,4},{6,7},{7,6},{8,9},{9,8},{10,11... | collective-permute-start | bytes 1572872 | tf_op jit(solution)/shard_map/ppermute | solution.py:461
  202.8 22.3 %copy-start.1 = (f32[16,2048]{1,0:T(8,128)S(1)}, f32[16,2048]{1,0:T(8,128)}, u32[]{:S(2)}) copy-start(f32[16,2048]{1,0:T(8,128)} %get-tuple-element.36.settled) | copy-start | bytes 393220
  202.8 22.3 %copy-start.4 = (f32[2048]{0:T(1024)S(1)}, f32[2048]{0:T(1024)}, u32[]{:S(2)}) copy-start(f32[2048]{0:T(1024)} %param.36) | copy-start | bytes 24580

commit v3 on v2

--- a/solution.py
+++ b/solution.py
@@ -76,6 +76,23 @@
     )
 
 
+def thirds(value):
+    high = value.astype(BF16)
+    rest = value - high.astype(F32)
+    middle = rest.astype(BF16)
+    return high, middle, (rest - middle.astype(F32)).astype(BF16)
+
+
+def sums_left(mask, value):
+    high, middle, low = thirds(value)
+    return fast_dot(mask, high) + (fast_dot(mask, middle) + fast_dot(mask, low))
+
+
+def sums_right(value, mask, dims=((1,), (0,))):
+    high, middle, low = thirds(value)
+    return fast_dot(high, mask, dims) + (fast_dot(middle, mask, dims) + fast_dot(low, mask, dims))
+
+
 def log_fading(pre):
     return (jnp.minimum(pre, 0.0) - jnp.log1p(jnp.exp(-jnp.abs(pre)))) / normalizer_sharpness
 
@@ -93,9 +110,9 @@
     size, length = k1.shape
     peers = spread.shape[0] // 24
     row, col = grid_of(length)
-    above = (row < col).astype(F32)
-    below = (row > col).astype(F32)
-    ones = jnp.ones((length, 128), F32)
+    above = (row < col).astype(F32).astype(BF16)
+    below = (row > col).astype(F32).astype(BF16)
+    ones = jnp.ones((length, 128), BF16)
 
     def put(value, kind, first):
         for n in range(value.shape[0] // peers):
@@ -105,17 +122,17 @@
 
     copies[0].wait()
     ahead, behind = log_fading(d1[0]), log_fading(d1[1])
-    fade_f = jnp.exp(exact_dot(ahead, below))
-    fade_b = jnp.exp(exact_dot(behind, above))
-    put(exact_dot(ahead, ones), 2, 0)
-    put(exact_dot(behind, ones), 3, 0)
+    fade_f = jnp.exp(sums_right(ahead, below))
+    fade_b = jnp.exp(sums_right(behind, above))
+    put(sums_right(ahead, ones), 2, 0)
+    put(sums_right(behind, ones), 3, 0)
     copies[1].wait()
     ahead, behind = log_fading(d2[0]), log_fading(d2[1])
-    wide_f = jnp.exp(exact_dot(above, ahead))
-    wide_b = jnp.exp(exact_dot(below, behind))
+    wide_f = jnp.exp(sums_left(above, ahead))
+    wide_b = jnp.exp(sums_left(below, behind))
     across = ((0,), (0,))
-    put(exact_dot(ahead, ones, across), 2, size // peers)
-    put(exact_dot(behind, ones, across), 3, size // peers)
+    put(sums_right(ahead, ones, across), 2, size // peers)
+    put(sums_right(behind, ones, across), 3, size // peers)
     copies[2].wait()
     copies[3].wait()
     key, value = k1[...].astype(F32), v1[...]
@@ -129,22 +146,22 @@
     pieces[...] = spread[...].astype(BF16)
 
 
-def pack_kernel(where, gate, up, down, one, two, stream, pack, proj, own, moves):
+def pack_kernel(gate, up, down, pack, moves):
     features, hidden = gate.shape[1:]
-    sources = [gate.at[0], up.at[0], one, two]
-    places = [
-        pack.at[:features, :hidden],
-        pack.at[:features, hidden:],
-        proj.at[:hidden, :],
-        proj.at[hidden:, :],
-    ]
+    sources = [gate.at[0], up.at[0]]
+    places = [pack.at[:features, :hidden], pack.at[:features, hidden:]]
     for n in range(down.shape[2] // (2 * hidden)):
         sources.append(down.at[0, :, 2 * hidden * n : 2 * hidden * (n + 1)])
         places.append(pack.at[features + hidden * n : features + hidden * (n + 1), :])
-    rows = own.shape[0]
-    sources.append(stream.at[pl.ds(pl.multiple_of(where[0] * rows, rows), rows), :])
-    places.append(own)
     for copy in fetched(sources, places, moves):
+        copy.wait()
+
+
+def gather_kernel(where, one, two, stream, proj, own, moves):
+    rows, hidden = own.shape[0], one.shape[0]
+    mine = stream.at[pl.ds(pl.multiple_of(where[0] * rows, rows), rows), :]
+    places = (proj.at[:hidden, :], proj.at[hidden:, :], own)
+    for copy in fetched((one, two, mine), places, moves):
         copy.wait()
 
 
@@ -187,8 +204,8 @@
         opened[:, place * 128 : (place + 1) * 128] = value * jax.nn.sigmoid(value) * gain[...]
     count = length // BLK
     row, col = grid_of(length)
-    upto = (col <= row).astype(F32)
-    since = (col >= row).astype(F32)
+    upto = (col <= row).astype(F32).astype(BF16)
+    since = (col >= row).astype(F32).astype(BF16)
     brow, bcol = grid_of(BLK)
     lower, upper = bcol <= brow, bcol >= brow
     on_last = ((1,), (1,))
@@ -205,16 +222,18 @@
         if size == DK_A:
             query, key, ahead, behind = query.T, key.T, ahead.T, behind.T
         ahead, behind = log_fading(ahead), log_fading(behind)
-        cum_f = exact_dot(upto, ahead)
-        cum_b = exact_dot(since, behind)
+        cum_f = sums_left(upto, ahead)
+        cum_b = sums_left(since, behind)
         reader[:, :size] = (query * jnp.exp(cum_f)).astype(BF16)
         reader[:, size:] = (query * jnp.exp(cum_b)).astype(BF16)
         sums = []
         for i in range(count):
             part = slice(i * BLK, (i + 1) * BLK)
-            own_f, own_b = ahead[part], behind[part]
-            local_f = exact_dot(upto[:BLK, :BLK], own_f)
-            local_b = exact_dot(since[:BLK, :BLK], own_b)
+            local_f, local_b = cum_f[part], cum_b[part]
+            if i > 0:
+                local_f = local_f - cum_f[i * BLK - 1 : i * BLK]
+            if i + 1 < count:
+                local_b = local_b - cum_b[(i + 1) * BLK : (i + 1) * BLK + 1]
             q_i, k_i = query[part], key[part]
             score_f = fast_dot(q_i * jnp.exp(local_f), k_i * jnp.exp(-local_f), on_last)
             score_b = fast_dot(q_i * jnp.exp(local_b), k_i * jnp.exp(-local_b), on_last)
@@ -355,7 +374,8 @@
             ]
 
 
-def dispatch_kernel(chosen, own, other, out, spread):
+def dispatch_kernel(chosen, own, other, side, far, out, side_here, far_here, spread, marks):
+    copies = fetched((side, far), (side_here, far_here), marks)
     wide = out.shape[1]
     each = SLOTS // SPLIT
     for part in range(LINES // each):
@@ -363,13 +383,12 @@
         both = jnp.concatenate([own[:, lanes], other[:, lanes]], axis=0)
         placed(spread, part, each, fast_dot(chosen[...], both))
     tighten(spread, out)
-
-
-def expert_kernel(
-    rows, own, near, side, far, out, spread, own_here, near_here, side_here, far_here, marks
-):
-    packs = (own_here, near_here, side_here, far_here)
-    copies = fetched((own, near, side, far), packs, marks)
+    for copy in copies:
+        copy.wait()
+
+
+def expert_kernel(rows, own, near, side, far, out, spread):
+    packs = (own, near, side, far)
     wide = rows.shape[1]
     hidden = own.shape[1] // 2
     each = SLOTS // SPLIT
@@ -378,8 +397,7 @@
     x = jnp.concatenate([taken(spread, part, each) for part in range(parts)], axis=1)
     features = parts * wide
     acts = []
-    for copy, pack in zip(copies, packs):
-        copy.wait()
+    for pack in packs:
         both = fast_dot(x, pack[:features, :])
         gate, upward = both[:, :hidden], both[:, hidden:]
         acts.append((gate * jax.nn.sigmoid(gate) * upward).astype(BF16))
@@ -398,6 +416,12 @@
     tighten(spread, out)
 
 
+def load_kernel(*refs):
+    count = len(refs) // 2
+    for copy in fetched(refs[:count], refs[count : 2 * count], refs[2 * count]):
+        copy.wait()
+
+
 def combine_kernel(weighted, *refs):
     returned, own, sent, spread = refs[:SPLIT], refs[SPLIT], refs[SPLIT + 1], refs[SPLIT + 2 :]
     half = own.shape[0]
@@ -435,15 +459,12 @@
     out[...] = (own[...] + got[...].astype(F32)).astype(BF16)
 
 
-def project_kernel(own, got, proj, other, out, proj_here, marks):
-    copies = fetched((proj,), (proj_here,), marks)
-    theirs = fast_dot(got[...], other[...])
-    copies[0].wait()
+def project_kernel(own, got, proj, other, out):
     width = out.shape[1]
     step = width // 4
     for n in range(4):
         lanes = slice(n * step, (n + 1) * step)
-        value = theirs[:, lanes] + fast_dot(own[...], proj_here[:, lanes])
+        value = fast_dot(got[...], other[:, lanes]) + fast_dot(own[...], proj[:, lanes])
         out[:, lanes] = value.astype(BF16)
 
 
@@ -558,7 +579,8 @@
         return held, pltpu.SemaphoreType.DMA((len(items),))
 
     early = (decay_one, decay_two, key_one, value_one, key_two, value_two)
-    moves = (expert_gate, expert_up, expert_down, proj_one, proj_two, stream)
+    weights = (expert_gate, expert_up, expert_down)
+    packed = (width + width // (2 * hidden) * hidden, 2 * hidden)
     held, marks = scratch(early)
     pieces_rows = 4 * keys
     blocks = width // (2 * hidden)
@@ -570,17 +592,22 @@
         scratch=held + [pltpu.VMEM((pieces_rows, 128), F32), marks],
     )
     arrived = exchange(pieces.reshape(peers, pieces_rows // peers, 128), SP)
-    pack, proj, stream_own = call(
+    pack = call(
         pack_kernel,
-        [
-            pltpu.HBM((width + blocks * hidden, 2 * hidden), BF16),
-            pltpu.HBM((2 * hidden, width), BF16),
-            shape((own_rows, width), BF16),
-        ],
+        pltpu.HBM(packed, BF16),
+        *weights,
+        far=range(len(weights)),
+        scratch=[pltpu.SemaphoreType.DMA((2 + blocks,))],
+    )
+    proj, stream_own = call(
+        gather_kernel,
+        [pltpu.HBM((2 * hidden, width), BF16), shape((own_rows, width), BF16)],
         tp_rank.reshape(1).astype(jnp.int32),
-        *moves,
-        far=range(1, 1 + len(moves)),
-        scratch=[pltpu.SemaphoreType.DMA((5 + blocks,))],
+        proj_one,
+        proj_two,
+        stream,
+        far=(1, 2, 3),
+        scratch=[pltpu.SemaphoreType.DMA((3,))],
     )
     near = swapped(pack, "b")
     side = swapped(pack, "c")
@@ -635,6 +662,13 @@
     )
     far = swapped(tied(near, heads_own), "c")
     heads_got = swapped(heads_sent, "c")
+    proj = call(
+        load_kernel,
+        shape((2 * hidden, width), BF16),
+        proj,
+        far=(0,),
+        scratch=[pltpu.SemaphoreType.DMA((1,))],
+    )
     part = call(
         project_kernel,
         pltpu.HBM((half, width), BF16),
@@ -642,8 +676,6 @@
         heads_got,
         proj,
         proj_other,
-        far=(2,),
-        scratch=[pltpu.VMEM((2 * hidden, width), BF16), pltpu.SemaphoreType.DMA((1,))],
     )
     attn = exchange(part.reshape(chips, own_rows, width), Y)
     settled, mine = call(
@@ -657,15 +689,26 @@
     moe_other = swapped(moe_own, "c")
     lines = peers * LINES
     spread = [pltpu.VMEM((wide // 128, lines, 128), F32)]
+    pack, near = call(
+        load_kernel,
+        [shape(packed, BF16)] * 2,
+        pack,
+        near,
+        far=(0, 1),
+        scratch=[pltpu.SemaphoreType.DMA((2,))],
+    )
     returned = []
     for turn in range(SPLIT):
-        outgoing = call(
+        outgoing, side, far = call(
             dispatch_kernel,
-            pltpu.HBM((lines, wide), BF16),
+            [pltpu.HBM((lines, wide), BF16)] + [shape(packed, BF16)] * 2,
             chosen[turn * each : (turn + 1) * each],
             moe_own,
             moe_other,
-            scratch=spread,
+            side,
+            far,
+            far=(3, 4),
+            scratch=spread + [pltpu.SemaphoreType.DMA((2,))],
         )
         complete = exchange(outgoing.reshape(peers, LINES, wide), SP)
         partial = call(
@@ -676,10 +719,7 @@
             near,
             side,
             far,
-            far=range(1, 5),
-            scratch=spread
-            + [pltpu.VMEM(pack.shape, BF16)] * 4
-            + [pltpu.SemaphoreType.DMA((4,))],
+            scratch=spread,
         )
         arrived = exchange(partial.reshape(peers, LINES, wide), SP)
         returned.append(arrived.reshape(lines, wide))

time: 227 us -> 207 us (0.912)
  blocking collectives: 110 us -> 88.1 us
  local copies, waits for them, and re-layouts: 0.93 us -> 8.61 us
  waiting for transfers between devices: 43.7 us -> 39.9 us
    all_to_all x4, blocking collectives: 110 us -> 88.1 us  [exchange(): return lax.all_to_all(pieces, axis, split_axis=0, concat_axis=0, tiled=True)]
    unnamed x18 -> x28, local copies, waits for them, and re-layouts: 0.93 us -> 8.61 us
    all_to_all x3, waiting for transfers between devices: 41.3 us -> 38.3 us  [exchange(): return lax.all_to_all(pieces, axis, split_axis=0, concat_axis=0, tiled=True)]
    pallas_call x13 -> x16, Pallas kernels: 27.7 us -> 27.6 us  [call(): pl.pallas_call(kernel, out_shape=shapes, in_specs=[pl.BlockSpec(memory_sp...]
  transfers between devices with their start and end apart: 10 -> 10, of which waited for: 5 -> 4; matrix products, arithmetic and copies ran while one was open for 0% -> 0% of each run, Pallas kernels for 6% -> 9%
where the time goes in v3:
time: 207 us; the launch traced here: 206 us
  blocking collectives  88.1 us (43%)
  starting transfers between devices  41.1 us (20%)
  waiting for transfers between devices  39.9 us (19%)
  Pallas kernels  27.6 us (13%)
  local copies, waits for them, and re-layouts  8.61 us (4%)
    all_to_all x4, blocking collectives, exchange(): return lax.all_to_all(pieces, axis, split_axis=0, concat_axis=0, tiled=True)  88.1 us
    all_to_all x3, waiting for transfers between devices, exchange(): return lax.all_to_all(pieces, axis, split_axis=0, concat_axis=0, tiled=True)  38.3 us
    pallas_call x16, Pallas kernels, call(): pl.pallas_call(kernel, out_shape=shapes, in_specs=[pl.BlockSpec(memory_sp...  27.6 us
    ppermute x7, starting transfers between devices, swapped(): return lax.ppermute(value, axis, SWAP)  27 us
    all_to_all x3, starting transfers between devices, exchange(): return lax.all_to_all(pieces, axis, split_axis=0, concat_axis=0, tiled=True)  14.1 us
    unnamed x28, local copies, waits for them, and re-layouts  8.61 us
  transfers between devices with their start and end apart: 10, of which 4 were waited for; matrix products, arithmetic and copies ran while one was open for 0% of the time, Pallas kernels for 9%

profile of v3, /device:TPU:1, one launch (start us, length us, event | category | flops | bytes accessed | tf_op | source)
XLA Modules:
  0.0 205.7 jit_solution(10361584846328205245)
XLA Ops:
  0.0 2.2 %shard_map.204 = (bf16[256,2048]{1,0:T(8,128)(2,1)}, bf16[16,2048]{1,0:T(8,128)(2,1)S(1)}) custom-call(s32[1]{0:T(128)} %bitcast.10.where, bf16[128,2048]{1,0:T(8,128)(2,1)} %one.1, bf16[128,2048]{1,0:T(8,128)(2,1)} %two.1, bf16[256,2048]{1,0:T(8,128)(2,1)} %stream.1), custom_call_target="tpu_custom_call" | custom-call | tf_op jit(solution)/shard_map/pallas_call | solution.py:34
  2.2 8.7 %collective-permute-start.1 = (bf16[256,2048]{1,0:T(8,128)(2,1)}, bf16[256,2048]{1,0:T(8,128)(2,1)S(1)}, u32[]{:S(2)}, u32[]{:S(2)}) collective-permute-start(bf16[256,2048]{1,0:T(8,128)(2,1)} %get-tuple-element.33.refs_0_), channel_id=1, source_target_pairs={{0,1},{1,0},{2,3},{3,2},{4,5},{5,4},{6,7},{7,6},{8,9},{9,8},{10,11... | collective-permute-start | bytes 3145736 | tf_op jit(solution)/shard_map/ppermute | solution.py:482
  11.0 2.6 %shard_map.208.refs_0_ = bf16[3072,256]{1,0:T(8,128)(2,1)} custom-call(bf16[1,2048,128]{2,1,0:T(8,128)(2,1)} %gate.1, bf16[1,2048,128]{2,1,0:T(8,128)(2,1)} %up.1, bf16[1,128,2048]{2,1,0:T(8,128)(2,1)} %down.1), custom_call_target="tpu_custom_call" | custom-call | tf_op jit(solution)/shard_map/pallas_call | solution.py:34
  13.6 1.9 collective-permute-start.4
  15.5 3.0 %shard_map.201 = bf16[768,128]{1,0:T(8,128)(2,1)} custom-call(f32[2,64,256]{2,1,0:T(8,128)} %bitcast.35, f32[2,256,128]{2,1,0:T(8,128)} %d2h.3, bf16[64,256]{1,0:T(8,128)(2,1)} %bitcast.37, bf16[256,128]{1,0:T(8,128)(2,1)} %v1h.3, bf16[256,128]{1,0:T(8,128)(2,1)} %k2h.3, bf16[256,128]{1,0:T(8,128)(2,1)} %v2h.3), custom_call_target="tpu_custom_call" | custom-call | tf_op jit(solution)/shard_map/pallas_call | solution.py:34
  18.5 19.4 %all_to_all.35.pieces = bf16[32,24,128]{2,1,0:T(8,128)(2,1)S(1)} all-to-all(bf16[32,24,128]{2,1,0:T(8,128)(2,1)} %bitcast.34), channel_id=1, replica_groups=mesh['z'=8,'x'=4,'p'=4,'b'=2,'c'=2] {'z','x'}, dimensions={0} | all-to-all | bytes 393216 | tf_op jit(solution)/shard_map/all_to_all | solution.py:478
  38.7 4.1 %all-to-all-start.1 = ((bf16[32,16,128]{2,1,0:T(8,128)(2,1)}), bf16[32,16,128]{2,1,0:T(8,128)(2,1)S(1)}, u32[]{:S(2)}, u32[]{:S(2)}) async-start(bf16[32,16,128]{2,1,0:T(8,128)(2,1)} %shard_map.202), calls=%async_computation.1 | async-start | bytes 262144 | tf_op jit(solution)/shard_map/all_to_all | solution.py:478
  42.9 3.1 %shard_map.200 = (f32[256,256]{1,0:T(8,128)S(1)}, bf16[256,128]{1,0:T(8,128)(2,1)S(1)}, bf16[256,256]{1,0:T(8,128)(2,1)S(1)}, f32[256,256]{1,0:T(8,128)S(1)}) custom-call(bf16[64,256]{1,0:T(8,128)(2,1)} %bitcast.39, bf16[64,256]{1,0:T(8,128)(2,1)} %bitcast.38, bf16[256,128]{1,0:T(8,128)(2,1)} %v1h.3, f32[2,64,256]{2,1,0:T(8,128)} %bitcast.36, ...), custom_call_target="tpu_custom_call" | custom-call | tf_op jit(solution)/shard_map/pallas_call | solution.py:34
  46.0 6.2 %all-to-all-done.1 = bf16[32,16,128]{2,1,0:T(8,128)(2,1)S(1)} async-done(((bf16[32,16,128]{2,1,0:T(8,128)(2,1)}), bf16[32,16,128]{2,1,0:T(8,128)(2,1)S(1)}, u32[]{:S(2)}, u32[]{:S(2)}) %all-to-all-start.1) | async-done | bytes 131104 | tf_op jit(solution)/shard_map/all_to_all | solution.py:478
  52.6 4.8 %collective-permute-start = (bf16[128,256]{1,0:T(8,128)(2,1)S(1)}, bf16[128,256]{1,0:T(8,128)(2,1)S(1)}, u32[]{:S(2)}, u32[]{:S(2)}) collective-permute-start(bf16[128,256]{1,0:T(8,128)(2,1)S(1)} %get-tuple-element.32), channel_id=1, source_target_pairs={{0,1},{1,0},{2,3},{3,2},{4,5},{5,4},{6,7},{7,6},{8,9},{9,8},{10,11... | collective-permute-start | bytes 196616 | tf_op jit(solution)/shard_map/ppermute | solution.py:482
  57.4 1.2 shard_map.205.proj
  58.6 1.3 shard_map.206
  59.9 6.1 %all-to-all-start.2 = ((bf16[8,16,2048]{2,1,0:T(8,128)(2,1)}), bf16[8,16,2048]{2,1,0:T(8,128)(2,1)S(1)}, u32[]{:S(2)}, u32[]{:S(2)}) async-start(bf16[8,16,2048]{2,1,0:T(8,128)(2,1)} %bitcast.31), calls=%async_computation.2 | async-start | bytes 1048576 | tf_op jit(solution)/shard_map/all_to_all | solution.py:478
  66.0 2.2 %collective-permute-start.3 = (bf16[3072,256]{1,0:T(8,128)(2,1)}, bf16[3072,256]{1,0:T(8,128)(2,1)}, u32[]{:S(2)}, u32[]{:S(2)}) collective-permute-start(bf16[3072,256]{1,0:T(8,128)(2,1)} %shard_map.208.refs_0_), channel_id=1, source_target_pairs={{0,1},{1,0},{2,3},{3,2},{4,5},{5,4},{6,7},{7,6},{8,9},{9,8},{10,11... | collective-permute-start | bytes 4718600 | tf_op jit(solution)/shard_map/ppermute | solution.py:482
  68.2 2.1 %collective-permute-start.5 = (bf16[3072,256]{1,0:T(8,128)(2,1)}, bf16[3072,256]{1,0:T(8,128)(2,1)}, u32[]{:S(2)}, u32[]{:S(2)}) collective-permute-start(bf16[3072,256]{1,0:T(8,128)(2,1)} %collective-permute-done.4.refs_1_), channel_id=1, source_target_pairs={{0,1},{1,0},{2,3},{3,2},{4,5},{5,4},{6,7},{7,6},{8,9},{9,8},{10,11... | collective-permute-start | bytes 4718600 | tf_op jit(solution)/shard_map/ppermute | solution.py:482
  70.3 13.7 %all-to-all-done.2.parts = bf16[8,16,2048]{2,1,0:T(8,128)(2,1)S(1)} async-done(((bf16[8,16,2048]{2,1,0:T(8,128)(2,1)}), bf16[8,16,2048]{2,1,0:T(8,128)(2,1)S(1)}, u32[]{:S(2)}, u32[]{:S(2)}) %all-to-all-start.2) | async-done | bytes 524320 | tf_op jit(solution)/shard_map/all_to_all | solution.py:478
  84.0 1.2 shard_map.207
  85.2 21.2 %all_to_all.36 = bf16[8,16,2048]{2,1,0:T(8,128)(2,1)S(1)} all-to-all(bf16[8,16,2048]{2,1,0:T(8,128)(2,1)} %get-tuple-element.35), channel_id=1, replica_groups=mesh['z'=8,'x'=4,'p'=4,'b'=2,'c'=2] {'p','b'}, dimensions={0} | all-to-all | bytes 1048576 | tf_op jit(solution)/shard_map/all_to_all | solution.py:478
  106.4 2.5 %collective-permute-start.2 = (bf16[128,2048]{1,0:T(8,128)(2,1)S(1)}, bf16[128,2048]{1,0:T(8,128)(2,1)S(1)}, u32[]{:S(2)}, u32[]{:S(2)}) collective-permute-start(bf16[128,2048]{1,0:T(8,128)(2,1)S(1)} %bitcast.22), channel_id=1, source_target_pairs={{0,1},{1,0},{2,3},{3,2},{4,5},{5,4},{6,7},{7,6},{8,9},{9,8},{10,11... | collective-permute-start | bytes 1572872 | tf_op jit(solution)/shard_map/ppermute | solution.py:482
  109.0 2.0 shard_map.199
  112.0 2.8 %shard_map.209 = (bf16[768,512]{1,0:T(8,128)(2,1)}, bf16[3072,256]{1,0:T(8,128)(2,1)S(1)}, bf16[3072,256]{1,0:T(8,128)(2,1)S(1)}) custom-call(bf16[192,256]{1,0:T(8,128)(2,1)S(1)} %copy-done.8, bf16[128,2048]{1,0:T(8,128)(2,1)S(1)} %bitcast.23, bf16[128,2048]{1,0:T(8,128)(2,1)S(1)} %collective-permute-done.2.other, ...), custom_call_target="tpu_custom_call" | custom-call | tf_op jit(solution)/shard_map/pallas_call | solution.py:34
  116.0 3.9 %all-to-all-start.4 = ((bf16[32,24,512]{2,1,0:T(8,128)(2,1)}), bf16[32,24,512]{2,1,0:T(8,128)(2,1)S(1)}, u32[]{:S(2)}, u32[]{:S(2)}) async-start(bf16[32,24,512]{2,1,0:T(8,128)(2,1)} %bitcast.33), calls=%async_computation.4 | async-start | bytes 1572864 | tf_op jit(solution)/shard_map/all_to_all | solution.py:478
  119.9 1.9 shard_map.210
  124.1 18.5 %all-to-all-done.4 = bf16[32,24,512]{2,1,0:T(8,128)(2,1)S(1)} async-done(((bf16[32,24,512]{2,1,0:T(8,128)(2,1)}), bf16[32,24,512]{2,1,0:T(8,128)(2,1)S(1)}, u32[]{:S(2)}, u32[]{:S(2)}) %all-to-all-start.4) | async-done | bytes 786464 | tf_op jit(solution)/shard_map/all_to_all | solution.py:478
  142.6 1.4 copy-done.1
  144.0 1.4 copy-done.3
  145.4 1.4 copy-done.5
  146.8 2.7 %shard_map.211 = bf16[768,512]{1,0:T(8,128)(2,1)} custom-call(bf16[768,512]{1,0:T(8,128)(2,1)S(1)} %bitcast.21, bf16[3072,256]{1,0:T(8,128)(2,1)S(1)} %copy-done.3, bf16[3072,256]{1,0:T(8,128)(2,1)S(1)} %copy-done.5, bf16[3072,256]{1,0:T(8,128)(2,1)S(1)} %get-tuple-element.40.side, bf16[3072,256]{1,0:T(8,128)(2,1)S(1)} %copy-done.1), custom_call_target="tpu_custom_call" | custom-call | tf_op jit(solution)/shard_map/pallas_call | solution.py:34
  149.5 26.1 %all_to_all.37 = bf16[32,24,512]{2,1,0:T(8,128)(2,1)S(1)} all-to-all(bf16[32,24,512]{2,1,0:T(8,128)(2,1)} %bitcast.30), channel_id=1, replica_groups=mesh['z'=8,'x'=4,'p'=4,'b'=2,'c'=2] {'z','x'}, dimensions={0} | all-to-all | bytes 1572864 | tf_op jit(solution)/shard_map/all_to_all | solution.py:478
  176.3 4.8 %collective-permute-start.6 = (bf16[128,2048]{1,0:T(8,128)(2,1)S(1)}, bf16[128,2048]{1,0:T(8,128)(2,1)S(1)}, u32[]{:S(2)}, u32[]{:S(2)}) collective-permute-start(bf16[128,2048]{1,0:T(8,128)(2,1)S(1)} %get-tuple-element.43), channel_id=1, source_target_pairs={{0,1},{1,0},{2,3},{3,2},{4,5},{5,4},{6,7},{7,6},{8,9},{9,8},{10,11... | collective-permute-start | bytes 1572872 | tf_op jit(solution)/shard_map/ppermute | solution.py:482
  181.0 1.5 collective-permute-done.6.got
  183.5 21.3 %all_to_all.38.parts = bf16[8,16,2048]{2,1,0:T(8,128)(2,1)S(1)} all-to-all(bf16[8,16,2048]{2,1,0:T(8,128)(2,1)} %bitcast.32), channel_id=1, replica_groups=mesh['z'=8,'x'=4,'p'=4,'b'=2,'c'=2] {'p','b'}, dimensions={0} | all-to-all | bytes 1048576 | tf_op jit(solution)/shard_map/all_to_all | solution.py:478
  (37 shorter events, 8.1 us)
Async XLA Ops:
  2.2 56.4 %collective-permute-start.1 = (bf16[256,2048]{1,0:T(8,128)(2,1)}, bf16[256,2048]{1,0:T(8,128)(2,1)S(1)}, u32[]{:S(2)}, u32[]{:S(2)}) collective-permute-start(bf16[256,2048]{1,0:T(8,128)(2,1)} %get-tuple-element.33.refs_0_), channel_id=1, source_target_pairs={{0,1},{1,0},{2,3},{3,2},{4,5},{5,4},{6,7},{7,6},{8,9},{9,8},{10,11... | collective-permute-start | bytes 3145736 | tf_op jit(solution)/shard_map/ppermute | solution.py:482
  13.5 29.3 %copy-start.13 = (f32[128]{0:T(128)S(1)}, f32[128]{0:T(128)}, u32[]{:S(2)}) copy-start(f32[128]{0:T(128)} %param.31) | copy-start | bytes 1540
  13.6 54.6 %collective-permute-start.4 = (bf16[3072,256]{1,0:T(8,128)(2,1)}, bf16[3072,256]{1,0:T(8,128)(2,1)}, u32[]{:S(2)}, u32[]{:S(2)}) collective-permute-start(bf16[3072,256]{1,0:T(8,128)(2,1)} %shard_map.208.refs_0_), channel_id=1, source_target_pairs={{0,2},{2,0},{1,3},{3,1},{4,6},{6,4},{5,7},{7,5},{8,10},{10,8},{9,1... | collective-permute-start | bytes 4718600 | tf_op jit(solution)/shard_map/ppermute | solution.py:482
  38.7 13.5 %all-to-all-start.1 = ((bf16[32,16,128]{2,1,0:T(8,128)(2,1)}), bf16[32,16,128]{2,1,0:T(8,128)(2,1)S(1)}, u32[]{:S(2)}, u32[]{:S(2)}) async-start(bf16[32,16,128]{2,1,0:T(8,128)(2,1)} %shard_map.202), calls=%async_computation.1 | async-start | bytes 262144 | tf_op jit(solution)/shard_map/all_to_all | solution.py:478
  52.6 6.0 %collective-permute-start = (bf16[128,256]{1,0:T(8,128)(2,1)S(1)}, bf16[128,256]{1,0:T(8,128)(2,1)S(1)}, u32[]{:S(2)}, u32[]{:S(2)}) collective-permute-start(bf16[128,256]{1,0:T(8,128)(2,1)S(1)} %get-tuple-element.32), channel_id=1, source_target_pairs={{0,1},{1,0},{2,3},{3,2},{4,5},{5,4},{6,7},{7,6},{8,9},{9,8},{10,11... | collective-permute-start | bytes 196616 | tf_op jit(solution)/shard_map/ppermute | solution.py:482
  58.6 25.4 %copy-start.9 = (f32[2048]{0:T(1024)S(1)}, f32[2048]{0:T(1024)}, u32[]{:S(2)}) copy-start(f32[2048]{0:T(1024)} %param.35) | copy-start | bytes 24580
  59.9 49.1 %copy-start.11 = (s32[256,2]{0,1:T(2,128)S(1)}, s32[256,2]{0,1:T(2,128)}, u32[]{:S(2)}) copy-start(s32[256,2]{0,1:T(2,128)} %param.37) | copy-start | bytes 6148
  59.9 49.1 %copy-start.12 = (f32[256,2]{0,1:T(2,128)S(1)}, f32[256,2]{0,1:T(2,128)}, u32[]{:S(2)}) copy-start(f32[256,2]{0,1:T(2,128)} %param.38) | copy-start | bytes 6148
  59.9 24.1 %all-to-all-start.2 = ((bf16[8,16,2048]{2,1,0:T(8,128)(2,1)}), bf16[8,16,2048]{2,1,0:T(8,128)(2,1)S(1)}, u32[]{:S(2)}, u32[]{:S(2)}) async-start(bf16[8,16,2048]{2,1,0:T(8,128)(2,1)} %bitcast.31), calls=%async_computation.2 | async-start | bytes 1048576 | tf_op jit(solution)/shard_map/all_to_all | solution.py:478
  66.0 45.1 %collective-permute-start.3 = (bf16[3072,256]{1,0:T(8,128)(2,1)}, bf16[3072,256]{1,0:T(8,128)(2,1)}, u32[]{:S(2)}, u32[]{:S(2)}) collective-permute-start(bf16[3072,256]{1,0:T(8,128)(2,1)} %shard_map.208.refs_0_), channel_id=1, source_target_pairs={{0,1},{1,0},{2,3},{3,2},{4,5},{5,4},{6,7},{7,6},{8,9},{9,8},{10,11... | collective-permute-start | bytes 4718600 | tf_op jit(solution)/shard_map/ppermute | solution.py:482
  68.2 42.9 %collective-permute-start.5 = (bf16[3072,256]{1,0:T(8,128)(2,1)}, bf16[3072,256]{1,0:T(8,128)(2,1)}, u32[]{:S(2)}, u32[]{:S(2)}) collective-permute-start(bf16[3072,256]{1,0:T(8,128)(2,1)} %collective-permute-done.4.refs_1_), channel_id=1, source_target_pairs={{0,1},{1,0},{2,3},{3,2},{4,5},{5,4},{6,7},{7,6},{8,9},{9,8},{10,11... | collective-permute-start | bytes 4718600 | tf_op jit(solution)/shard_map/ppermute | solution.py:482
  106.4 4.6 %collective-permute-start.2 = (bf16[128,2048]{1,0:T(8,128)(2,1)S(1)}, bf16[128,2048]{1,0:T(8,128)(2,1)S(1)}, u32[]{:S(2)}, u32[]{:S(2)}) collective-permute-start(bf16[128,2048]{1,0:T(8,128)(2,1)S(1)} %bitcast.22), channel_id=1, source_target_pairs={{0,1},{1,0},{2,3},{3,2},{4,5},{5,4},{6,7},{7,6},{8,9},{9,8},{10,11... | collective-permute-start | bytes 1572872 | tf_op jit(solution)/shard_map/ppermute | solution.py:482
  111.1 0.9 copy-start.8
  114.8 1.2 copy-start
  116.0 26.6 %all-to-all-start.4 = ((bf16[32,24,512]{2,1,0:T(8,128)(2,1)}), bf16[32,24,512]{2,1,0:T(8,128)(2,1)S(1)}, u32[]{:S(2)}, u32[]{:S(2)}) async-start(bf16[32,24,512]{2,1,0:T(8,128)(2,1)} %bitcast.33), calls=%async_computation.4 | async-start | bytes 1572864 | tf_op jit(solution)/shard_map/all_to_all | solution.py:478
  121.8 1.2 copy-start.2
  123.0 1.2 copy-start.4
  142.6 1.4 copy-start.1
  144.0 1.4 copy-start.3
  145.4 1.4 copy-start.5
  149.5 26.1 %copy-start.6 = (bf16[256,192]{1,0:T(8,128)(2,1)S(1)}, bf16[256,192]{1,0:T(8,128)(2,1)}, u32[]{:S(2)}) copy-start(bf16[256,192]{1,0:T(8,128)(2,1)} %get-tuple-element.25.weighted) | copy-start | bytes 294916
  176.3 6.3 %collective-permute-start.6 = (bf16[128,2048]{1,0:T(8,128)(2,1)S(1)}, bf16[128,2048]{1,0:T(8,128)(2,1)S(1)}, u32[]{:S(2)}, u32[]{:S(2)}) collective-permute-start(bf16[128,2048]{1,0:T(8,128)(2,1)S(1)} %get-tuple-element.43), channel_id=1, source_target_pairs={{0,1},{1,0},{2,3},{3,2},{4,5},{5,4},{6,7},{7,6},{8,9},{9,8},{10,11... | collective-permute-start | bytes 1572872 | tf_op jit(solution)/shard_map/ppermute | solution.py:482
  182.6 22.2 %copy-start.7 = (f32[16,2048]{1,0:T(8,128)S(1)}, f32[16,2048]{1,0:T(8,128)}, u32[]{:S(2)}) copy-start(f32[16,2048]{1,0:T(8,128)} %get-tuple-element.44.settled) | copy-start | bytes 393220
  182.6 22.2 %copy-start.10 = (f32[2048]{0:T(1024)S(1)}, f32[2048]{0:T(1024)}, u32[]{:S(2)}) copy-start(f32[2048]{0:T(1024)} %param.36) | copy-start | bytes 24580

commit v4 on v3

--- a/solution.py
+++ b/solution.py
@@ -374,8 +374,8 @@
             ]
 
 
-def dispatch_kernel(chosen, own, other, side, far, out, side_here, far_here, spread, marks):
-    copies = fetched((side, far), (side_here, far_here), marks)
+def dispatch_kernel(chosen, own, other, far, out, far_here, spread, marks):
+    copies = fetched((far,), (far_here,), marks)
     wide = out.shape[1]
     each = SLOTS // SPLIT
     for part in range(LINES // each):
@@ -594,7 +594,7 @@
     arrived = exchange(pieces.reshape(peers, pieces_rows // peers, 128), SP)
     pack = call(
         pack_kernel,
-        pltpu.HBM(packed, BF16),
+        shape(packed, BF16),
         *weights,
         far=range(len(weights)),
         scratch=[pltpu.SemaphoreType.DMA((2 + blocks,))],
@@ -689,26 +689,25 @@
     moe_other = swapped(moe_own, "c")
     lines = peers * LINES
     spread = [pltpu.VMEM((wide // 128, lines, 128), F32)]
-    pack, near = call(
+    near, side = call(
         load_kernel,
         [shape(packed, BF16)] * 2,
-        pack,
         near,
+        side,
         far=(0, 1),
         scratch=[pltpu.SemaphoreType.DMA((2,))],
     )
     returned = []
     for turn in range(SPLIT):
-        outgoing, side, far = call(
+        outgoing, far = call(
             dispatch_kernel,
-            [pltpu.HBM((lines, wide), BF16)] + [shape(packed, BF16)] * 2,
+            [pltpu.HBM((lines, wide), BF16), shape(packed, BF16)],
             chosen[turn * each : (turn + 1) * each],
             moe_own,
             moe_other,
-            side,
             far,
-            far=(3, 4),
-            scratch=spread + [pltpu.SemaphoreType.DMA((2,))],
+            far=(3,),
+            scratch=spread + [pltpu.SemaphoreType.DMA((1,))],
         )
         complete = exchange(outgoing.reshape(peers, LINES, wide), SP)
         partial = call(

time: 207 us -> 206 us (level)
  no operation moved by 1% of the time
where the time goes in v4:
time: 206 us; the launch traced here: 205 us
  blocking collectives  88.6 us (43%)
  starting transfers between devices  41 us (20%)
  waiting for transfers between devices  40.7 us (20%)
  Pallas kernels  26 us (13%)
  local copies, waits for them, and re-layouts  8.62 us (4%)
    all_to_all x4, blocking collectives, exchange(): return lax.all_to_all(pieces, axis, split_axis=0, concat_axis=0, tiled=True)  88.6 us
    all_to_all x3, waiting for transfers between devices, exchange(): return lax.all_to_all(pieces, axis, split_axis=0, concat_axis=0, tiled=True)  39.2 us
    ppermute x7, starting transfers between devices, swapped(): return lax.ppermute(value, axis, SWAP)  26.9 us
    pallas_call x16, Pallas kernels, call(): pl.pallas_call(kernel, out_shape=shapes, in_specs=[pl.BlockSpec(memory_sp...  26 us
    all_to_all x3, starting transfers between devices, exchange(): return lax.all_to_all(pieces, axis, split_axis=0, concat_axis=0, tiled=True)  14.1 us
    unnamed x28, local copies, waits for them, and re-layouts  8.62 us
  transfers between devices with their start and end apart: 10, of which 4 were waited for; matrix products, arithmetic and copies ran while one was open for 0% of the time, Pallas kernels for 9%

profile of v4, /device:TPU:1, one launch (start us, length us, event | category | flops | bytes accessed | tf_op | source)
XLA Modules:
  0.0 205.2 jit_solution(11315400620539308170)
XLA Ops:
  0.0 2.2 %shard_map.204 = (bf16[256,2048]{1,0:T(8,128)(2,1)}, bf16[16,2048]{1,0:T(8,128)(2,1)S(1)}) custom-call(s32[1]{0:T(128)} %bitcast.10.where, bf16[128,2048]{1,0:T(8,128)(2,1)} %one.1, bf16[128,2048]{1,0:T(8,128)(2,1)} %two.1, bf16[256,2048]{1,0:T(8,128)(2,1)} %stream.1), custom_call_target="tpu_custom_call" | custom-call | tf_op jit(solution)/shard_map/pallas_call | solution.py:34
  2.2 8.7 %collective-permute-start.1 = (bf16[256,2048]{1,0:T(8,128)(2,1)}, bf16[256,2048]{1,0:T(8,128)(2,1)S(1)}, u32[]{:S(2)}, u32[]{:S(2)}) collective-permute-start(bf16[256,2048]{1,0:T(8,128)(2,1)} %get-tuple-element.32.refs_0_), channel_id=1, source_target_pairs={{0,1},{1,0},{2,3},{3,2},{4,5},{5,4},{6,7},{7,6},{8,9},{9,8},{10,11... | collective-permute-start | bytes 3145736 | tf_op jit(solution)/shard_map/ppermute | solution.py:482
  11.0 1.4 shard_map.208.own
  12.4 1.9 collective-permute-start.3
  14.3 3.0 %shard_map.201 = bf16[768,128]{1,0:T(8,128)(2,1)} custom-call(f32[2,64,256]{2,1,0:T(8,128)} %bitcast.35, f32[2,256,128]{2,1,0:T(8,128)} %d2h.3, bf16[64,256]{1,0:T(8,128)(2,1)} %bitcast.37, bf16[256,128]{1,0:T(8,128)(2,1)} %v1h.3, bf16[256,128]{1,0:T(8,128)(2,1)} %k2h.3, bf16[256,128]{1,0:T(8,128)(2,1)} %v2h.3), custom_call_target="tpu_custom_call" | custom-call | tf_op jit(solution)/shard_map/pallas_call | solution.py:34
  17.3 19.4 %all_to_all.35.pieces = bf16[32,24,128]{2,1,0:T(8,128)(2,1)S(1)} all-to-all(bf16[32,24,128]{2,1,0:T(8,128)(2,1)} %bitcast.34), channel_id=1, replica_groups=mesh['z'=8,'x'=4,'p'=4,'b'=2,'c'=2] {'z','x'}, dimensions={0} | all-to-all | bytes 393216 | tf_op jit(solution)/shard_map/all_to_all | solution.py:478
  37.6 4.1 %all-to-all-start.1 = ((bf16[32,16,128]{2,1,0:T(8,128)(2,1)}), bf16[32,16,128]{2,1,0:T(8,128)(2,1)S(1)}, u32[]{:S(2)}, u32[]{:S(2)}) async-start(bf16[32,16,128]{2,1,0:T(8,128)(2,1)} %shard_map.202), calls=%async_computation.1 | async-start | bytes 262144 | tf_op jit(solution)/shard_map/all_to_all | solution.py:478
  41.7 3.1 %shard_map.200 = (f32[256,256]{1,0:T(8,128)S(1)}, bf16[256,128]{1,0:T(8,128)(2,1)S(1)}, bf16[256,256]{1,0:T(8,128)(2,1)S(1)}, f32[256,256]{1,0:T(8,128)S(1)}) custom-call(bf16[64,256]{1,0:T(8,128)(2,1)} %bitcast.39, bf16[64,256]{1,0:T(8,128)(2,1)} %bitcast.38, bf16[256,128]{1,0:T(8,128)(2,1)} %v1h.3, f32[2,64,256]{2,1,0:T(8,128)} %bitcast.36, ...), custom_call_target="tpu_custom_call" | custom-call | tf_op jit(solution)/shard_map/pallas_call | solution.py:34
  44.8 6.2 %all-to-all-done.1 = bf16[32,16,128]{2,1,0:T(8,128)(2,1)S(1)} async-done(((bf16[32,16,128]{2,1,0:T(8,128)(2,1)}), bf16[32,16,128]{2,1,0:T(8,128)(2,1)S(1)}, u32[]{:S(2)}, u32[]{:S(2)}) %all-to-all-start.1) | async-done | bytes 131104 | tf_op jit(solution)/shard_map/all_to_all | solution.py:478
  51.4 4.8 %collective-permute-start = (bf16[128,256]{1,0:T(8,128)(2,1)S(1)}, bf16[128,256]{1,0:T(8,128)(2,1)S(1)}, u32[]{:S(2)}, u32[]{:S(2)}) collective-permute-start(bf16[128,256]{1,0:T(8,128)(2,1)S(1)} %get-tuple-element.31), channel_id=1, source_target_pairs={{0,1},{1,0},{2,3},{3,2},{4,5},{5,4},{6,7},{7,6},{8,9},{9,8},{10,11... | collective-permute-start | bytes 196616 | tf_op jit(solution)/shard_map/ppermute | solution.py:482
  56.2 1.2 shard_map.205.proj
  57.5 1.3 shard_map.206
  58.7 6.1 %all-to-all-start.2 = ((bf16[8,16,2048]{2,1,0:T(8,128)(2,1)}), bf16[8,16,2048]{2,1,0:T(8,128)(2,1)S(1)}, u32[]{:S(2)}, u32[]{:S(2)}) async-start(bf16[8,16,2048]{2,1,0:T(8,128)(2,1)} %bitcast.31), calls=%async_computation.2 | async-start | bytes 1048576 | tf_op jit(solution)/shard_map/all_to_all | solution.py:478
  64.8 2.2 %collective-permute-start.4 = (bf16[3072,256]{1,0:T(8,128)(2,1)}, bf16[3072,256]{1,0:T(8,128)(2,1)}, u32[]{:S(2)}, u32[]{:S(2)}) collective-permute-start(bf16[3072,256]{1,0:T(8,128)(2,1)} %collective-permute-done.3.refs_0_), channel_id=1, source_target_pairs={{0,1},{1,0},{2,3},{3,2},{4,5},{5,4},{6,7},{7,6},{8,9},{9,8},{10,11... | collective-permute-start | bytes 4718600 | tf_op jit(solution)/shard_map/ppermute | solution.py:482
  67.0 15.8 %all-to-all-done.2.parts = bf16[8,16,2048]{2,1,0:T(8,128)(2,1)S(1)} async-done(((bf16[8,16,2048]{2,1,0:T(8,128)(2,1)}), bf16[8,16,2048]{2,1,0:T(8,128)(2,1)S(1)}, u32[]{:S(2)}, u32[]{:S(2)}) %all-to-all-start.2) | async-done | bytes 524320 | tf_op jit(solution)/shard_map/all_to_all | solution.py:478
  84.0 21.2 %all_to_all.36 = bf16[8,16,2048]{2,1,0:T(8,128)(2,1)S(1)} all-to-all(bf16[8,16,2048]{2,1,0:T(8,128)(2,1)} %get-tuple-element.34), channel_id=1, replica_groups=mesh['z'=8,'x'=4,'p'=4,'b'=2,'c'=2] {'p','b'}, dimensions={0} | all-to-all | bytes 1048576 | tf_op jit(solution)/shard_map/all_to_all | solution.py:478
  105.2 2.5 %collective-permute-start.2 = (bf16[128,2048]{1,0:T(8,128)(2,1)S(1)}, bf16[128,2048]{1,0:T(8,128)(2,1)S(1)}, u32[]{:S(2)}, u32[]{:S(2)}) collective-permute-start(bf16[128,2048]{1,0:T(8,128)(2,1)S(1)} %bitcast.22), channel_id=1, source_target_pairs={{0,1},{1,0},{2,3},{3,2},{4,5},{5,4},{6,7},{7,6},{8,9},{9,8},{10,11... | collective-permute-start | bytes 1572872 | tf_op jit(solution)/shard_map/ppermute | solution.py:482
  107.7 1.9 collective-permute-start.5
  109.7 2.1 shard_map.199
  112.7 2.4 %shard_map.209 = (bf16[768,512]{1,0:T(8,128)(2,1)}, bf16[3072,256]{1,0:T(8,128)(2,1)S(1)}) custom-call(bf16[192,256]{1,0:T(8,128)(2,1)S(1)} %copy-done.8, bf16[128,2048]{1,0:T(8,128)(2,1)S(1)} %bitcast.23, bf16[128,2048]{1,0:T(8,128)(2,1)S(1)} %collective-permute-done.2.other, bf16[3072,256]{1,0:T(8,128)(2,1)} %collective-permute-done.4.far), custom_call_target="tpu_custom_call" | custom-call | tf_op jit(solution)/shard_map/pallas_call | solution.py:34
  116.2 3.9 %all-to-all-start.4 = ((bf16[32,24,512]{2,1,0:T(8,128)(2,1)}), bf16[32,24,512]{2,1,0:T(8,128)(2,1)S(1)}, u32[]{:S(2)}, u32[]{:S(2)}) async-start(bf16[32,24,512]{2,1,0:T(8,128)(2,1)} %bitcast.33), calls=%async_computation.4 | async-start | bytes 1572864 | tf_op jit(solution)/shard_map/all_to_all | solution.py:478
  120.2 1.9 shard_map.210
  122.1 1.2 copy-done.2
  124.4 17.1 %all-to-all-done.4 = bf16[32,24,512]{2,1,0:T(8,128)(2,1)S(1)} async-done(((bf16[32,24,512]{2,1,0:T(8,128)(2,1)}), bf16[32,24,512]{2,1,0:T(8,128)(2,1)S(1)}, u32[]{:S(2)}, u32[]{:S(2)}) %all-to-all-start.4) | async-done | bytes 786464 | tf_op jit(solution)/shard_map/all_to_all | solution.py:478
  141.6 1.4 copy-done.1
  143.0 1.4 copy-done.3
  144.4 1.4 copy-done.5
  145.8 2.7 %shard_map.211 = bf16[768,512]{1,0:T(8,128)(2,1)} custom-call(bf16[768,512]{1,0:T(8,128)(2,1)S(1)} %bitcast.21, bf16[3072,256]{1,0:T(8,128)(2,1)S(1)} %shard_map.208.own, bf16[3072,256]{1,0:T(8,128)(2,1)S(1)} %copy-done.3, bf16[3072,256]{1,0:T(8,128)(2,1)S(1)} %copy-done.5, bf16[3072,256]{1,0:T(8,128)(2,1)S(1)} %copy-done.1), custom_call_target="tpu_custom_call" | custom-call | tf_op jit(solution)/shard_map/pallas_call | solution.py:34
  148.5 26.6 %all_to_all.37 = bf16[32,24,512]{2,1,0:T(8,128)(2,1)S(1)} all-to-all(bf16[32,24,512]{2,1,0:T(8,128)(2,1)} %bitcast.30), channel_id=1, replica_groups=mesh['z'=8,'x'=4,'p'=4,'b'=2,'c'=2] {'z','x'}, dimensions={0} | all-to-all | bytes 1572864 | tf_op jit(solution)/shard_map/all_to_all | solution.py:478
  175.7 4.8 %collective-permute-start.6 = (bf16[128,2048]{1,0:T(8,128)(2,1)S(1)}, bf16[128,2048]{1,0:T(8,128)(2,1)S(1)}, u32[]{:S(2)}, u32[]{:S(2)}) collective-permute-start(bf16[128,2048]{1,0:T(8,128)(2,1)S(1)} %get-tuple-element.41), channel_id=1, source_target_pairs={{0,1},{1,0},{2,3},{3,2},{4,5},{5,4},{6,7},{7,6},{8,9},{9,8},{10,11... | collective-permute-start | bytes 1572872 | tf_op jit(solution)/shard_map/ppermute | solution.py:482
  180.6 1.5 collective-permute-done.6.got
  183.0 21.3 %all_to_all.38.parts = bf16[8,16,2048]{2,1,0:T(8,128)(2,1)S(1)} all-to-all(bf16[8,16,2048]{2,1,0:T(8,128)(2,1)} %bitcast.32), channel_id=1, replica_groups=mesh['z'=8,'x'=4,'p'=4,'b'=2,'c'=2] {'p','b'}, dimensions={0} | all-to-all | bytes 1048576 | tf_op jit(solution)/shard_map/all_to_all | solution.py:478
  (37 shorter events, 8.0 us)
Async XLA Ops:
  2.2 55.2 %collective-permute-start.1 = (bf16[256,2048]{1,0:T(8,128)(2,1)}, bf16[256,2048]{1,0:T(8,128)(2,1)S(1)}, u32[]{:S(2)}, u32[]{:S(2)}) collective-permute-start(bf16[256,2048]{1,0:T(8,128)(2,1)} %get-tuple-element.32.refs_0_), channel_id=1, source_target_pairs={{0,1},{1,0},{2,3},{3,2},{4,5},{5,4},{6,7},{7,6},{8,9},{9,8},{10,11... | collective-permute-start | bytes 3145736 | tf_op jit(solution)/shard_map/ppermute | solution.py:482
  12.4 29.3 %copy-start.13 = (f32[128]{0:T(128)S(1)}, f32[128]{0:T(128)}, u32[]{:S(2)}) copy-start(f32[128]{0:T(128)} %param.31) | copy-start | bytes 1540
  12.4 52.4 %collective-permute-start.3 = (bf16[3072,256]{1,0:T(8,128)(2,1)S(1)}, bf16[3072,256]{1,0:T(8,128)(2,1)}, u32[]{:S(2)}, u32[]{:S(2)}) collective-permute-start(bf16[3072,256]{1,0:T(8,128)(2,1)S(1)} %shard_map.208.own), channel_id=1, source_target_pairs={{0,2},{2,0},{1,3},{3,1},{4,6},{6,4},{5,7},{7,5},{8,10},{10,8},{9,1... | collective-permute-start | bytes 4718600 | tf_op jit(solution)/shard_map/ppermute | solution.py:482
  37.6 13.5 %all-to-all-start.1 = ((bf16[32,16,128]{2,1,0:T(8,128)(2,1)}), bf16[32,16,128]{2,1,0:T(8,128)(2,1)S(1)}, u32[]{:S(2)}, u32[]{:S(2)}) async-start(bf16[32,16,128]{2,1,0:T(8,128)(2,1)} %shard_map.202), calls=%async_computation.1 | async-start | bytes 262144 | tf_op jit(solution)/shard_map/all_to_all | solution.py:478
  51.4 6.0 %collective-permute-start = (bf16[128,256]{1,0:T(8,128)(2,1)S(1)}, bf16[128,256]{1,0:T(8,128)(2,1)S(1)}, u32[]{:S(2)}, u32[]{:S(2)}) collective-permute-start(bf16[128,256]{1,0:T(8,128)(2,1)S(1)} %get-tuple-element.31), channel_id=1, source_target_pairs={{0,1},{1,0},{2,3},{3,2},{4,5},{5,4},{6,7},{7,6},{8,9},{9,8},{10,11... | collective-permute-start | bytes 196616 | tf_op jit(solution)/shard_map/ppermute | solution.py:482
  57.5 25.4 %copy-start.9 = (f32[2048]{0:T(1024)S(1)}, f32[2048]{0:T(1024)}, u32[]{:S(2)}) copy-start(f32[2048]{0:T(1024)} %param.35) | copy-start | bytes 24580
  58.7 51.0 %copy-start.11 = (s32[256,2]{0,1:T(2,128)S(1)}, s32[256,2]{0,1:T(2,128)}, u32[]{:S(2)}) copy-start(s32[256,2]{0,1:T(2,128)} %param.37) | copy-start | bytes 6148
  58.7 51.0 %copy-start.12 = (f32[256,2]{0,1:T(2,128)S(1)}, f32[256,2]{0,1:T(2,128)}, u32[]{:S(2)}) copy-start(f32[256,2]{0,1:T(2,128)} %param.38) | copy-start | bytes 6148
  58.7 24.1 %all-to-all-start.2 = ((bf16[8,16,2048]{2,1,0:T(8,128)(2,1)}), bf16[8,16,2048]{2,1,0:T(8,128)(2,1)S(1)}, u32[]{:S(2)}, u32[]{:S(2)}) async-start(bf16[8,16,2048]{2,1,0:T(8,128)(2,1)} %bitcast.31), calls=%async_computation.2 | async-start | bytes 1048576 | tf_op jit(solution)/shard_map/all_to_all | solution.py:478
  64.8 47.0 %collective-permute-start.4 = (bf16[3072,256]{1,0:T(8,128)(2,1)}, bf16[3072,256]{1,0:T(8,128)(2,1)}, u32[]{:S(2)}, u32[]{:S(2)}) collective-permute-start(bf16[3072,256]{1,0:T(8,128)(2,1)} %collective-permute-done.3.refs_0_), channel_id=1, source_target_pairs={{0,1},{1,0},{2,3},{3,2},{4,5},{5,4},{6,7},{7,6},{8,9},{9,8},{10,11... | collective-permute-start | bytes 4718600 | tf_op jit(solution)/shard_map/ppermute | solution.py:482
  105.2 6.6 %collective-permute-start.2 = (bf16[128,2048]{1,0:T(8,128)(2,1)S(1)}, bf16[128,2048]{1,0:T(8,128)(2,1)S(1)}, u32[]{:S(2)}, u32[]{:S(2)}) collective-permute-start(bf16[128,2048]{1,0:T(8,128)(2,1)S(1)} %bitcast.22), channel_id=1, source_target_pairs={{0,1},{1,0},{2,3},{3,2},{4,5},{5,4},{6,7},{7,6},{8,9},{9,8},{10,11... | collective-permute-start | bytes 1572872 | tf_op jit(solution)/shard_map/ppermute | solution.py:482
  107.7 12.4 %collective-permute-start.5 = (bf16[3072,256]{1,0:T(8,128)(2,1)S(1)}, bf16[3072,256]{1,0:T(8,128)(2,1)}, u32[]{:S(2)}, u32[]{:S(2)}) collective-permute-start(bf16[3072,256]{1,0:T(8,128)(2,1)S(1)} %shard_map.208.own), channel_id=1, source_target_pairs={{0,1},{1,0},{2,3},{3,2},{4,5},{5,4},{6,7},{7,6},{8,9},{9,8},{10,11... | collective-permute-start | bytes 4718600 | tf_op jit(solution)/shard_map/ppermute | solution.py:482
  111.8 0.9 copy-start.8
  115.1 1.2 copy-start
  116.2 25.3 %all-to-all-start.4 = ((bf16[32,24,512]{2,1,0:T(8,128)(2,1)}), bf16[32,24,512]{2,1,0:T(8,128)(2,1)S(1)}, u32[]{:S(2)}, u32[]{:S(2)}) async-start(bf16[32,24,512]{2,1,0:T(8,128)(2,1)} %bitcast.33), calls=%async_computation.4 | async-start | bytes 1572864 | tf_op jit(solution)/shard_map/all_to_all | solution.py:478
  122.1 1.2 copy-start.2
  123.3 1.2 copy-start.4
  141.5 1.4 copy-start.1
  143.0 1.4 copy-start.3
  144.4 1.4 copy-start.5
  148.5 26.6 %copy-start.6 = (bf16[256,192]{1,0:T(8,128)(2,1)S(1)}, bf16[256,192]{1,0:T(8,128)(2,1)}, u32[]{:S(2)}) copy-start(bf16[256,192]{1,0:T(8,128)(2,1)} %get-tuple-element.24.weighted) | copy-start | bytes 294916
  175.7 6.4 %collective-permute-start.6 = (bf16[128,2048]{1,0:T(8,128)(2,1)S(1)}, bf16[128,2048]{1,0:T(8,128)(2,1)S(1)}, u32[]{:S(2)}, u32[]{:S(2)}) collective-permute-start(bf16[128,2048]{1,0:T(8,128)(2,1)S(1)} %get-tuple-element.41), channel_id=1, source_target_pairs={{0,1},{1,0},{2,3},{3,2},{4,5},{5,4},{6,7},{7,6},{8,9},{9,8},{10,11... | collective-permute-start | bytes 1572872 | tf_op jit(solution)/shard_map/ppermute | solution.py:482
  182.1 22.2 %copy-start.7 = (f32[16,2048]{1,0:T(8,128)S(1)}, f32[16,2048]{1,0:T(8,128)}, u32[]{:S(2)}) copy-start(f32[16,2048]{1,0:T(8,128)} %get-tuple-element.42.settled) | copy-start | bytes 393220
  182.1 22.2 %copy-start.10 = (f32[2048]{0:T(1024)S(1)}, f32[2048]{0:T(1024)}, u32[]{:S(2)}) copy-start(f32[2048]{0:T(1024)} %param.36) | copy-start | bytes 24580
